TPU v7x, 256 devices: a whole 4x4x8 slice. The times are simulated.
256 devices in a mesh: ep: 128 (over z, y, x), tp: 2 (over core).
Axes of the slice: x: 4, y: 4, z: 8, core: 2. Of those that a mesh axis runs over, the one named last changes fastest.
Arguments:
- tokens: bfloat16 [2048, 2048], P('ep', 'tp'), may hold values from -6 to 6
- state: float32 [2048, 4, 128, 128], P('ep', 'tp'), may hold values from -4 to 4
- norm_mix: float32 [2048], replicated, may hold values from 0.1 to 1.9
- w_query: bfloat16 [2048, 512], P(None, 'tp'), may hold values from -0.125 to 0.125
- w_key: bfloat16 [2048, 512], P(None, 'tp'), may hold values from -0.125 to 0.125
- w_value: bfloat16 [2048, 512], P(None, 'tp'), may hold values from -0.125 to 0.125
- w_out: bfloat16 [512, 2048], P('tp'), may hold values from -0.25 to 0.25
- norm_ffn: float32 [2048], P('tp'), may hold values from 0.1 to 1.9
- gate_vector: bfloat16 [2048], P('tp'), may hold values from -0.125 to 0.125
- dense_gate: bfloat16 [2048, 2816], P('tp', 'ep'), may hold values from -0.125 to 0.125
- dense_up: bfloat16 [2048, 2816], P('tp', 'ep'), may hold values from -0.125 to 0.125
- dense_down: bfloat16 [2816, 2048], P('ep', 'tp'), may hold values from -0.109375 to 0.109375
- exp_gate: bfloat16 [128, 2048, 176], P('ep', None, 'tp'), may hold values from -0.125 to 0.125
- exp_up: bfloat16 [128, 2048, 176], P('ep', None, 'tp'), may hold values from -0.125 to 0.125
- exp_down: bfloat16 [128, 176, 2048], P('ep', 'tp'), may hold values from -0.109375 to 0.109375
- routes: int32 [2048, 2], P('ep'), may hold values from 0 to 7, all different within a row; in each aligned block of 16 rows (0 to 15, 16 to 31, ...) at most 5 rows name the same one
- route_w: bfloat16 [2048, 2], P('ep'), may hold values from 0.099609375 to 1
Outputs:
- mixed: bfloat16 [2048, 2048], P('ep', 'tp')
- new_state: float32 [2048, 4, 128, 128], P('ep', 'tp')
Inputs may be any that keep to these rules, and one draw needn't show every extreme that they name: `routes`: each row names 2 different experts. Within the rows of one device (aligned blocks of 16 rows) no expert is named by more than 5 rows, a bound that some blocks reach.
All inputs are finite; a program needn't handle non-finite values.
Results may differ from a plain program's by a relative error of at most 0.014.
Values may be sent and summed in bfloat16 or wider, within the bound.
A program may use at most 128 MiB of HBM per device.

v0:
```python
import functools

import jax
import jax.numpy as jnp
from jax import lax
from jax.experimental import pallas as pl
from jax.experimental.pallas import tpu as pltpu
from jax.sharding import PartitionSpec as P

EXPERTS = 8
ROWS = 256
epsilon = 1e-06
MESH = pl.DeviceIdType.MESH
F32 = jnp.float32
BF16 = jnp.bfloat16


def dot(a, b):
    return jnp.dot(a, b, preferred_element_type=F32)


def dot_t(a, b):
    return lax.dot_general(a, b, (((1,), (1,)), ((), ())), preferred_element_type=F32)


def silu(v):
    return v / (1.0 + jnp.exp(-v))


def kernel(
    A,
    B,
    tokens_h,
    norm_mix_h,
    routes_h,
    route_w_h,
    norm_ffn_h,
    gate_vec_h,
    state,
    w_query,
    w_key,
    w_value,
    w_out,
    dense_gate,
    dense_up,
    dense_down,
    exp_gate,
    exp_up,
    exp_down,
    mixed,
    ns,
    tokens,
    norm_mix,
    routes,
    route_w,
    norm_ffn,
    gate_vec,
    tok_p,
    gvec_p,
    wq,
    wk,
    wv,
    wo_o,
    wo_p,
    dg,
    du,
    dd,
    eg,
    eu,
    ed,
    st,
    ho_o,
    ho_p,
    aux,
    xo,
    xp,
    y0,
    yx_s,
    yx_r,
    ys,
    rsx,
    zs,
    rsz,
    lsem,
    psem_s,
    psem_r,
    axz_s,
    axz_r,
    axx_s,
    axx_r,
    gz_s,
    gz_r,
    gx_s,
    gx_r,
    gp_s,
    gp_r,
    yx_ss,
    yx_rs,
    rx_s,
    rx_r,
    rz_s,
    rz_r,
):
    R, H = tokens.shape
    D = 2 * H
    heads, hs = state.shape[1], state.shape[2]
    HW = heads * hs
    n = A * B
    me = lax.axis_index("ep")
    tp = lax.axis_index("tp")
    z, xy = me // B, me % B
    other = 1 - tp
    expert = me // (n // EXPERTS)
    partner = {"ep": me, "tp": other}
    xpeer = [{"ep": z * B + (xy + j) % B, "tp": tp} for j in range(B)]
    zpeer = [{"ep": ((z + i) % A) * B + xy, "tp": tp} for i in range(A)]

    own_at = pl.multiple_of(tp * H, H)
    oth_at = pl.multiple_of(other * H, H)
    own, oth = pl.ds(own_at, H), pl.ds(oth_at, H)

    sent = []

    def remote(src, dst, s, r, dev):
        copy = pltpu.make_async_remote_copy(
            src_ref=src, dst_ref=dst, send_sem=s, recv_sem=r, device_id=dev, device_id_type=MESH
        )
        copy.start()
        sent.append(copy)
        return copy

    local = {}

    def load(name, k, src, dst):
        copy = pltpu.make_async_copy(src, dst, lsem.at[k])
        copy.start()
        local[name] = copy

    small = (
        (tokens_h, tokens),
        (norm_mix_h, norm_mix),
        (routes_h, routes),
        (route_w_h, route_w),
        (norm_ffn_h, norm_ffn),
        (gate_vec_h, gate_vec),
    )
    barrier = pltpu.get_barrier_semaphore()
    for dev in [partner] + xpeer[1:] + zpeer[1:]:
        pl.semaphore_signal(barrier, inc=1, device_id=dev, device_id_type=MESH)

    for t, (src, dst) in enumerate(small):
        load(f"s{t}", 19 + t, src, dst)
    for t, (src, dst) in enumerate(((w_query, wq), (w_key, wk), (w_value, wv))):
        load(f"p{t}o", 2 * t, src.at[own, :], dst.at[0])
        load(f"p{t}p", 2 * t + 1, src.at[oth, :], dst.at[1])
    load("st", 6, state, st)
    load("wo0", 7, w_out.at[:, own], wo_o.at[0])
    load("wo1", 8, w_out.at[:, oth], wo_o.at[1])
    for t in (2, 3):
        local[f"s{t}"].wait()
    row_id = lax.broadcasted_iota(jnp.int32, (EXPERTS, R), 0)
    wt = jnp.zeros((EXPERTS, R), F32)
    named = routes[...]
    gains = route_w[...].astype(F32)
    for t in range(routes.shape[0]):
        wt = wt + jnp.where(row_id == named[t : t + 1, :], gains[t : t + 1, :], 0.0)
    wt = jnp.concatenate([wt, jnp.zeros((EXPERTS, 128 - R), F32)], axis=1)
    wt = jnp.concatenate([wt, jnp.zeros((128 - EXPERTS, 128), F32)], axis=0)
    aux[0, 0] = wt.T[:R].astype(BF16)

    for t in (0, 1, 4, 5):
        local[f"s{t}"].wait()
    pl.semaphore_wait(barrier, 1 + (B - 1) + (A - 1))

    c_tok = remote(tokens, tok_p, psem_s.at[0], psem_r.at[0], partner)
    c_ext = remote(gate_vec, gvec_p, psem_s.at[1], psem_r.at[1], partner)
    c_wo0 = remote(w_out.at[:, oth], wo_p.at[0], psem_s.at[2], psem_r.at[2], partner)
    c_wo1 = remote(w_out.at[:, own], wo_p.at[1], psem_s.at[3], psem_r.at[3], partner)
    c_dg = remote(dense_gate, dg.at[1], psem_s.at[4], psem_r.at[4], partner)
    c_du = remote(dense_up, du.at[1], psem_s.at[5], psem_r.at[5], partner)
    load("dg", 9, dense_gate, dg.at[0])
    load("du", 10, dense_up, du.at[0])
    load("dd", 11, dense_down, dd)
    load("eg0", 12, exp_gate.at[:, own], eg.at[0])
    load("eu0", 13, exp_up.at[:, own], eu.at[0])
    load("eg1", 14, exp_gate.at[:, oth], eg.at[1])
    load("eu1", 15, exp_up.at[:, oth], eu.at[1])
    load("ed1", 16, exp_down.at[0, :, oth], ed.at[1])
    load("ed0", 17, exp_down.at[0, :, own], ed.at[0])
    c_axz = [None] + [
        remote(aux.at[0, 0], aux.at[A - i, 0], axz_s.at[i], axz_r.at[A - i], zpeer[i])
        for i in range(1, A)
    ]

    tok_f = tokens[...].astype(F32)
    c_tok.wait_recv()
    tok_pf = tok_p[...].astype(F32)
    total = jnp.sum(tok_f * tok_f, axis=1, keepdims=True) + jnp.sum(
        tok_pf * tok_pf, axis=1, keepdims=True
    )
    scale = lax.rsqrt(total / D + epsilon)
    gain_o = norm_mix[:, own]
    gain_p = norm_mix[:, oth]
    nx_o = (tok_f * scale * gain_o).astype(BF16)
    nx_p = (tok_pf * scale * gain_p).astype(BF16)
    proj = []
    for t, w in enumerate((wq, wk, wv)):
        local[f"p{t}o"].wait()
        part = dot(nx_o, w[0])
        local[f"p{t}p"].wait()
        proj.append((part + dot(nx_p, w[1])).astype(BF16).astype(F32))
    q, k, v = proj
    k = k * hs ** (-0.5)
    pad = jnp.zeros((128 - R, HW), F32)
    q_t = jnp.concatenate([q, pad], axis=0).T
    k_t = jnp.concatenate([k, pad], axis=0).T
    head_id = tp * heads
    local["st"].wait()
    decays = []
    for h in range(heads):
        cols = slice(h * hs, (h + 1) * hs)
        idv = jnp.zeros((1, 128), F32) + (head_id + h).astype(F32)
        decay = 1.0 - jnp.exp2(-3.0 - 2.0 * idv)
        decays.append(decay)
        rows = []
        for s in range(R):
            rows.append(jnp.sum(st[s, h] * q_t[cols, s : s + 1], axis=0, keepdims=True))
        qs = jnp.concatenate(rows, axis=0)
        qk = jnp.sum(q[:, cols] * k[:, cols], axis=1, keepdims=True)
        read = decay * qs + qk * v[:, cols]
        centre = jnp.mean(read, axis=1, keepdims=True)
        dev = read - centre
        spread = jnp.mean(dev * dev, axis=1, keepdims=True)
        ho_o[:, cols] = (dev * lax.rsqrt(spread + epsilon)).astype(BF16)
    c_ho = remote(ho_o, ho_p, psem_s.at[6], psem_r.at[6], partner)
    ho = ho_o[...]
    local["wo0"].wait()
    local["wo1"].wait()
    a_o = dot(ho, wo_o[0]).astype(BF16).astype(F32)
    a_p = dot(ho, wo_o[1]).astype(BF16).astype(F32)
    c_wo0.wait_recv()
    c_wo1.wait_recv()
    c_ho.wait_recv()
    hp = ho_p[...]
    a_o = a_o + dot(hp, wo_p[0]).astype(BF16).astype(F32)
    a_p = a_p + dot(hp, wo_p[1]).astype(BF16).astype(F32)
    after = (tok_f + a_o).astype(BF16).astype(F32)
    after_p = (tok_pf + a_p).astype(BF16).astype(F32)
    squares = jnp.sum(after * after, axis=1, keepdims=True) + jnp.sum(
        after_p * after_p, axis=1, keepdims=True
    )
    xo[0, 0] = (after * lax.rsqrt(squares / D + epsilon) * norm_ffn[...]).astype(BF16)

    c_gz = [None] * A
    c_gx = {}
    c_gp = {}
    for i in range(1, A):
        c_gz[i] = remote(xo.at[0, 0], xo.at[A - i, 0], gz_s.at[i], gz_r.at[A - i], zpeer[i])

    def spread_block(i):
        for j in range(1, B):
            c_gx[i, j] = remote(
                xo.at[i, 0], xo.at[i, B - j], gx_s.at[i, j], gx_r.at[i, B - j], xpeer[j]
            )

    def to_partner(i, j):
        c_gp[i, j] = remote(xo.at[i, j], xp.at[i, j], gp_s.at[i, j], gp_r.at[i, j], partner)

    spread_block(0)
    to_partner(0, 0)
    c_axx = {}
    for i in range(A):
        if i > 0:
            c_axz[A - i].wait_recv()
        for j in range(1, B):
            c_axx[i, j] = remote(
                aux.at[i, 0], aux.at[i, B - j], axx_s.at[i, j], axx_r.at[i, B - j], xpeer[j]
            )

    for h in range(heads):
        cols = slice(h * hs, (h + 1) * hs)
        for s in range(R):
            ns[s, h] = decays[h] * st[s, h] + k_t[cols, s : s + 1] * v[s : s + 1, cols]

    order = sorted(range(A), key=lambda i: min(i, A - i))
    for i in order[1:]:
        c_gz[A - i].wait_recv()
        spread_block(i)
        to_partner(i, 0)

    c_ext.wait_recv()
    for name in ("dg", "du", "dd", "eg0", "eu0", "eg1", "eu1", "ed1", "ed0"):
        local[name].wait()
    c_dg.wait_recv()
    c_du.wait_recv()
    group = max(1, min(A, ROWS // (B * R)))
    rows = group * B * R

    def gate_row(ref):
        part = ref[...].astype(F32)
        return jnp.concatenate([part[r : r + 1] for r in range(H // 128)], axis=1)

    gvec_o = gate_row(gate_vec)
    gvec_q = gate_row(gvec_p)
    lanes = lax.broadcasted_iota(jnp.int32, (rows, 128), 1)
    c_yx = {}
    c_rx = {}
    c_rz = {}

    def arrive(i):
        for j in range(1, B):
            c_gx[i, B - j].wait_recv()
            to_partner(i, j)

    def experts(g):
        slots = range(g * group, (g + 1) * group)
        at = slice(g * group, (g + 1) * group)
        for i in slots:
            for j in range(1, B):
                c_axx[i, B - j].wait_recv()
        x_o = xo[at].reshape(rows, H)
        gate = dot_t(x_o, eg[0])
        up = dot_t(x_o, eu[0])
        d_gate = dot_t(x_o, dg[0])
        d_up = dot_t(x_o, du[0])
        logit = jnp.sum(x_o.astype(F32) * gvec_o, axis=1, keepdims=True)
        for i in slots:
            for j in range(B):
                c_gp[i, j].wait_recv()
        x_p = xp[at].reshape(rows, H)
        gate = gate + dot_t(x_p, eg[1])
        up = up + dot_t(x_p, eu[1])
        d_gate = d_gate + dot_t(x_p, dg[1])
        d_up = d_up + dot_t(x_p, du[1])
        logit = logit + jnp.sum(x_p.astype(F32) * gvec_q, axis=1, keepdims=True)
        table = aux[at].reshape(rows, 128).astype(F32)
        weight = jnp.sum(jnp.where(lanes == expert, table, 0.0), axis=1, keepdims=True)
        hidden = (silu(gate) * up).astype(BF16)
        d_hidden = (1.0 / (1.0 + jnp.exp(-logit)) * silu(d_gate) * d_up).astype(BF16)
        yx_s[at] = (weight * dot(hidden, ed[1])).astype(BF16).reshape(group, B, R, H)
        span = pl.ds(g * group, group)
        c_yx[g] = remote(yx_s.at[span], yx_r.at[span], yx_ss.at[g], yx_rs.at[g], partner)
        y = weight * dot(hidden, ed[0]) + dot(d_hidden, dd[...])
        y0[at] = y.reshape(group, B, R, H)

    def plane_send(g):
        c_yx[g].wait_recv()
        for i in range(g * group, (g + 1) * group):
            y = y0[i] + yx_r[i].astype(F32)
            y0[i, 0] = y[0]
            ys[i] = y.astype(BF16)
            for j in range(1, B):
                c_rx[i, j] = remote(
                    ys.at[i, j], rsx.at[i, B - j], rx_s.at[i, j], rx_r.at[i, B - j], xpeer[j]
                )

    def plane_sum(g):
        for i in range(g * group, (g + 1) * group):
            total = y0[i, 0]
            for j in range(1, B):
                c_rx[i, B - j].wait_recv()
                total = total + rsx[i, j].astype(F32)
            if i == 0:
                y0[0, 0] = total
            else:
                zs[i] = total.astype(BF16)
                c_rz[i] = remote(zs.at[i], rsz.at[A - i], rz_s.at[i], rz_r.at[A - i], zpeer[i])

    turns = A // group
    for t in range(turns + 2):
        if t < turns:
            for i in order:
                if i // group == t:
                    arrive(i)
            experts(t)
        if 1 <= t <= turns:
            plane_send(t - 1)
        if t >= 2:
            plane_sum(t - 2)

    result = after + y0[0, 0]
    for i in range(1, A):
        c_rz[A - i].wait_recv()
        result = result + rsz[i].astype(F32)
    mixed[...] = result.astype(BF16)
    for copy in sent:
        copy.wait_send()


def store(a_in, b_in, a_out, b_out, sems):
    first = pltpu.make_async_copy(b_in, b_out, sems.at[0])
    second = pltpu.make_async_copy(a_in, a_out, sems.at[1])
    first.start()
    second.start()
    first.wait()
    second.wait()


def body(
    tokens,
    state,
    norm_mix,
    w_query,
    w_key,
    w_value,
    w_out,
    norm_ffn,
    gate_vector,
    dense_gate,
    dense_up,
    dense_down,
    exp_gate,
    exp_up,
    exp_down,
    routes,
    route_w,
):
    n = lax.axis_size("ep")
    A = 1
    while (2 * A) * (2 * A) <= n:
        A = 2 * A
    B = n // A
    R, H = tokens.shape
    heads, hs = state.shape[1], state.shape[2]
    HW = heads * hs
    FE = exp_gate.shape[2]
    FD = dense_gate.shape[1]
    vm = pl.BlockSpec(memory_space=pltpu.VMEM)
    hbm = pl.BlockSpec(memory_space=pltpu.HBM)
    V = pltpu.VMEM
    sem = lambda *shape: pltpu.SemaphoreType.DMA(shape)
    operands = (
        tokens,
        norm_mix.reshape(1, -1),
        routes.T,
        route_w.T,
        norm_ffn.reshape(1, -1),
        gate_vector.reshape(-1, 128),
        state,
        w_query,
        w_key,
        w_value,
        w_out,
        dense_gate.T,
        dense_up.T,
        dense_down,
        exp_gate[0].T,
        exp_up[0].T,
        exp_down,
    )
    held = [pltpu.with_memory_space_constraint(x, pltpu.HBM) for x in operands]
    mixed, new_state = pl.pallas_call(
        functools.partial(kernel, A, B),
        out_shape=(pltpu.VMEM((R, H), BF16), pltpu.VMEM(state.shape, F32)),
        in_specs=[hbm] * 17,
        out_specs=(vm, vm),
        scratch_shapes=[
            V((R, H), BF16),
            V((1, 2 * H), F32),
            V((routes.shape[1], R), jnp.int32),
            V((routes.shape[1], R), BF16),
            V((1, H), F32),
            V((H // 128, 128), BF16),
            V((R, H), BF16),
            V((H // 128, 128), BF16),
            V((2, H, HW), BF16),
            V((2, H, HW), BF16),
            V((2, H, HW), BF16),
            V((2, HW, H), BF16),
            V((2, HW, H), BF16),
            V((2, FD, H), BF16),
            V((2, FD, H), BF16),
            V((FD, H), BF16),
            V((2, FE, H), BF16),
            V((2, FE, H), BF16),
            V((2, FE, H), BF16),
            V(state.shape, F32),
            V((R, HW), BF16),
            V((R, HW), BF16),
            V((A, B, R, 128), BF16),
            V((A, B, R, H), BF16),
            V((A, B, R, H), BF16),
            V((A, B, R, H), F32),
            V((A, B, R, H), BF16),
            V((A, B, R, H), BF16),
            V((A, B, R, H), BF16),
            V((A, B, R, H), BF16),
            V((A, R, H), BF16),
            V((A, R, H), BF16),
            sem(25),
            sem(7),
            sem(7),
            sem(A),
            sem(A),
            sem(A, B),
            sem(A, B),
            sem(A),
            sem(A),
            sem(A, B),
            sem(A, B),
            sem(A, B),
            sem(A, B),
            sem(A),
            sem(A),
            sem(A, B),
            sem(A, B),
            sem(A),
            sem(A),
        ],
        compiler_params=pltpu.CompilerParams(
            collective_id=0, has_side_effects=True, vmem_limit_bytes=50 * 1024 * 1024
        ),
        name="layer",
    )(
        *held
    )
    return pl.pallas_call(
        store,
        out_shape=(
            jax.ShapeDtypeStruct((R, H), BF16),
            jax.ShapeDtypeStruct(state.shape, F32),
        ),
        in_specs=[vm, vm],
        out_specs=(hbm, hbm),
        scratch_shapes=[sem(2)],
        name="store",
    )(
        pltpu.with_memory_space_constraint(mixed, pltpu.VMEM),
        pltpu.with_memory_space_constraint(new_state, pltpu.VMEM),
    )


def solution(mesh):
    return jax.shard_map(
        body,
        mesh=mesh,
        in_specs=(
            P("ep", "tp"),
            P("ep", "tp", None, None),
            P(),
            P(None, "tp"),
            P(None, "tp"),
            P(None, "tp"),
            P("tp", None),
            P("tp"),
            P("tp"),
            P("tp", "ep"),
            P("tp", "ep"),
            P("ep", "tp"),
            P("ep", None, "tp"),
            P("ep", None, "tp"),
            P("ep", "tp", None),
            P("ep", None),
            P("ep", None),
        ),
        out_specs=(P("ep", "tp"), P("ep", "tp", None, None)),
        check_vma=False,
    )
```

profile of v0, /device:TPU:1, one launch (start us, length us, event | category | flops | bytes accessed | tf_op | source)
XLA Modules:
  0.0 134.2 jit_solution(10684008607738142647)
XLA Ops:
  0.6 132.0 %layer.1 = (bf16[16,1024]{1,0:T(8,128)(2,1)S(1)}, f32[16,2,128,128]{3,2,1,0:T(8,128)S(1)}) custom-call(bf16[16,1024]{1,0:T(8,128)(2,1)} %tokens_h.1, f32[1,2048]{1,0:T(1,128)} %bitcast.17, s32[2,16]{1,0:T(2,128)} %bitcast.20, bf16[2,16]{1,0:T(2,128)(2,1)} %bitcast.21, f32[1,1024]{1,0:T(1,128)} %bitcast.18, bf16[8,128]{1,0:T(8,128)(2,1)} %bitcast.19, ...), custom_call_target="tpu_custom_call" | custom-call | tf_op jit(solution)/shard_map/layer/pallas_call | solution.py:452
  132.7 1.3 store.1
where the time goes:
time: 136 us; the launch traced here: 134 us
  Pallas kernels  133 us (98%)
    pallas_call x1, Pallas kernels, body(): pl.pallas_call(functools.partial(kernel, A, B), out_shape=(pltpu.VMEM((R,...  132 us

commit v1 on v0

v1 whole, which is shorter than its diff:
```python
import functools

import jax
import jax.numpy as jnp
from jax import lax
from jax.experimental import pallas as pl
from jax.experimental.pallas import tpu as pltpu
from jax.sharding import PartitionSpec as P

EXPERTS = 8
CAP = 5
SLOT = 8
SIDE = 4
PLANE = SIDE * SIDE
TRIPS = ((0, 1, 7), (2, 6, 3), (5, 4))
epsilon = 1e-06
MESH = pl.DeviceIdType.MESH
F32 = jnp.float32
BF16 = jnp.bfloat16


def dot(a, b):
    return jnp.dot(a, b, preferred_element_type=F32)


def dot_t(a, b):
    return lax.dot_general(a, b, (((1,), (1,)), ((), ())), preferred_element_type=F32)


def silu(v):
    return v / (1.0 + jnp.exp(-v))


def iota(shape, dim):
    return lax.broadcasted_iota(jnp.int32, shape, dim)


def kernel(
    tokens_h,
    norm_mix_h,
    routes_h,
    route_w_h,
    norm_ffn_h,
    gate_vec_h,
    state,
    w_query,
    w_key,
    w_value,
    w_out,
    dense_gate,
    dense_up,
    dense_down,
    exp_gate,
    exp_up,
    exp_down,
    mixed,
    ns,
    tokens,
    norm_mix,
    routes,
    route_w,
    norm_ffn,
    gate_vec,
    tok_p,
    wq,
    wk,
    wv,
    wo_o,
    wo_p,
    eg,
    eu,
    ed,
    st,
    ho_o,
    ho_p,
    sel_m,
    comb_m,
    lg_s,
    lg_r,
    wbuf,
    wdg,
    wdu,
    wdd,
    w1,
    w2,
    xs,
    zr,
    xz,
    xe,
    pe_o,
    pe_s,
    pe_r,
    pd_o,
    pd_s,
    pd_r,
    y32,
    yb,
    rb,
    rd,
    rs,
    rf,
    sa,
    sb,
    ab,
    ad,
    ax,
    af,
    zs,
    zret,
    yz0,
    yzs,
    yzr,
    lsem,
    ssem,
    rsem,
):
    R, H = tokens.shape
    D = 2 * H
    heads, hs = state.shape[1], state.shape[2]
    HW = heads * hs
    FE = eg.shape[1]
    FD = wbuf.shape[2]
    Z = EXPERTS
    me = lax.axis_index("ep")
    tp = lax.axis_index("tp")
    other = 1 - tp
    z, y_at, x_at = me // PLANE, (me // SIDE) % SIDE, me % SIDE

    def in_plane(dy, dx):
        return {
            "ep": z * PLANE + ((y_at + dy + SIDE) % SIDE) * SIDE + (x_at + dx + SIDE) % SIDE,
            "tp": tp,
        }

    first = {d: in_plane(tp * d, other * d) for d in (1, -1)}
    second = {d: in_plane(other * d, tp * d) for d in (1, -1)}
    zpeer = [{"ep": ((z + i) % Z) * PLANE + me % PLANE, "tp": tp} for i in range(Z)]
    partner = {"ep": me, "tp": other}

    def place(p):
        turned = (p % SIDE) * SIDE + p // SIDE
        return p + tp * (turned - p)

    own = pl.ds(pl.multiple_of(tp * H, H), H)
    oth = pl.ds(pl.multiple_of(other * H, H), H)

    sent = []

    def remote(src, dst, dev):
        k = len(sent)
        copy = pltpu.make_async_remote_copy(
            src_ref=src,
            dst_ref=dst,
            send_sem=ssem.at[k],
            recv_sem=rsem.at[k],
            device_id=dev,
            device_id_type=MESH,
        )
        copy.start()
        sent.append(copy)
        return copy

    local = {}

    def load(name, src, dst):
        copy = pltpu.make_async_copy(src, dst, lsem.at[len(local)])
        copy.start()
        local[name] = copy

    class Gather:
        def __init__(self, buf, via):
            self.buf, self.via = buf, via
            self.up, self.down = {}, {}

        def spread(self, a):
            at = self.buf.at
            self.up[a] = remote(at[a], at[3 * SIDE + a], second[1])
            self.down[a] = remote(at[a], at[SIDE + a], second[-1])

        def start(self):
            at = self.buf.at
            self.f_up = remote(at[0], at[3], first[1])
            self.f_down = remote(at[0], at[1], first[-1])
            self.spread(0)

        def one(self):
            at = self.buf.at
            self.f_up.wait_recv()
            if self.via > 0:
                self.f_two = remote(at[3], at[2], first[1])
            self.spread(3)
            self.f_down.wait_recv()
            if self.via < 0:
                self.f_two = remote(at[1], at[2], first[-1])
            self.spread(1)

        def two(self):
            self.f_two.wait_recv()
            self.spread(2)

        def relay(self, todo):
            at = self.buf.at
            for a in todo:
                self.up[a].wait_recv()
                if a in (0, 1):
                    self.up[a + SIDE] = remote(at[3 * SIDE + a], at[2 * SIDE + a], second[1])
                self.down[a].wait_recv()
                if a in (2, 3):
                    self.up[a + SIDE] = remote(at[SIDE + a], at[2 * SIDE + a], second[-1])

        def finish(self):
            for a in range(SIDE):
                self.up[a + SIDE].wait_recv()

    small = (
        (tokens_h, tokens),
        (norm_mix_h, norm_mix),
        (routes_h, routes),
        (route_w_h, route_w),
        (norm_ffn_h, norm_ffn),
        (gate_vec_h, gate_vec),
    )
    barrier = pltpu.get_barrier_semaphore()
    greeted = [partner, first[1], first[-1], second[1], second[-1]] + zpeer[1:]
    for dev in greeted:
        pl.semaphore_signal(barrier, inc=1, device_id=dev, device_id_type=MESH)

    for t, (src, dst) in enumerate(small):
        load(f"s{t}", src, dst)
    for t, src in enumerate((dense_gate, dense_up, dense_down)):
        load(f"d{t}", src, wbuf.at[0, t])
    for t, (src, dst) in enumerate(((w_query, wq), (w_key, wk), (w_value, wv))):
        load(f"p{t}o", src.at[own, :], dst.at[0])
        load(f"p{t}p", src.at[oth, :], dst.at[1])
    load("st", state, st)
    load("wo0", w_out.at[:, own], wo_o.at[0])
    load("wo1", w_out.at[:, oth], wo_o.at[1])
    load("eg", exp_gate.at[:, own], eg.at[tp])
    load("eu", exp_up.at[:, own], eu.at[tp])
    load("ed", exp_down.at[0, :, own], ed.at[tp])

    for t in (2, 3):
        local[f"s{t}"].wait()
    row_id = iota((EXPERTS, R), 0)
    wt = jnp.zeros((EXPERTS, R), F32)
    member = jnp.zeros((EXPERTS, R), F32)
    named = routes[...]
    gains = route_w[...].astype(F32)
    for t in range(routes.shape[0]):
        hit = row_id == named[t : t + 1, :]
        wt = wt + jnp.where(hit, gains[t : t + 1, :], 0.0)
        member = member + jnp.where(hit, 1.0, 0.0)
    blank = jnp.zeros((EXPERTS, 128 - R), F32)
    wt = jnp.concatenate([wt, blank], axis=1)
    member = jnp.concatenate([member, blank], axis=1)
    before = jnp.where(iota((128, 128), 0) < iota((128, 128), 1), 1.0, 0.0).astype(BF16)
    rank = dot(member.astype(BF16), before)
    slot_id = iota((SLOT, 128), 0).astype(F32)
    picks, scaled = [], []
    for e in range(EXPERTS):
        pick = jnp.where(rank[e : e + 1] == slot_id, member[e : e + 1], 0.0)
        picks.append(pick)
        scaled.append(pick * wt[e : e + 1])
    sel_m[...] = jnp.concatenate(picks, axis=0)
    scaled.append(jnp.zeros((128 - EXPERTS * SLOT, 128), F32))
    comb_m[...] = jnp.concatenate(scaled, axis=0).T[:R]

    for t in (0, 1, 4, 5):
        local[f"s{t}"].wait()
    for t in range(3):
        local[f"d{t}"].wait()
    pl.semaphore_wait(barrier, len(greeted))

    c_tok = remote(tokens, tok_p, partner)
    weights = Gather(wbuf, 1)
    weights.start()
    c_wo0 = remote(w_out.at[:, oth], wo_p.at[0], partner)
    c_wo1 = remote(w_out.at[:, own], wo_p.at[1], partner)
    c_eg = remote(exp_gate.at[:, oth], eg.at[tp], partner)
    c_eu = remote(exp_up.at[:, oth], eu.at[tp], partner)
    c_ed = remote(exp_down.at[0, :, oth], ed.at[tp], partner)

    tok_f = tokens[...].astype(F32)
    c_tok.wait_recv()
    tok_pf = tok_p[...].astype(F32)
    total = jnp.sum(tok_f * tok_f, axis=1, keepdims=True) + jnp.sum(
        tok_pf * tok_pf, axis=1, keepdims=True
    )
    scale = lax.rsqrt(total / D + epsilon)
    gain_o = norm_mix[:, own]
    gain_p = norm_mix[:, oth]
    nx_o = (tok_f * scale * gain_o).astype(BF16)
    nx_p = (tok_pf * scale * gain_p).astype(BF16)
    proj = []
    for t, w in enumerate((wq, wk, wv)):
        local[f"p{t}o"].wait()
        part = dot(nx_o, w[0])
        local[f"p{t}p"].wait()
        proj.append((part + dot(nx_p, w[1])).astype(BF16).astype(F32))
    q, k, v = proj
    k = k * hs ** (-0.5)
    pad = jnp.zeros((128 - R, HW), F32)
    q_t = jnp.concatenate([q, pad], axis=0).T
    k_t = jnp.concatenate([k, pad], axis=0).T
    head_id = tp * heads
    local["st"].wait()
    decays = []
    for h in range(heads):
        cols = slice(h * hs, (h + 1) * hs)
        idv = jnp.zeros((1, 128), F32) + (head_id + h).astype(F32)
        decay = 1.0 - jnp.exp2(-3.0 - 2.0 * idv)
        decays.append(decay)
        rows = []
        for s in range(R):
            rows.append(jnp.sum(st[s, h] * q_t[cols, s : s + 1], axis=0, keepdims=True))
        qs = jnp.concatenate(rows, axis=0)
        qk = jnp.sum(q[:, cols] * k[:, cols], axis=1, keepdims=True)
        read = decay * qs + qk * v[:, cols]
        centre = jnp.mean(read, axis=1, keepdims=True)
        dev = read - centre
        spread = jnp.mean(dev * dev, axis=1, keepdims=True)
        ho_o[:, cols] = (dev * lax.rsqrt(spread + epsilon)).astype(BF16)
    c_ho = remote(ho_o, ho_p, partner)
    weights.one()
    ho = ho_o[...]
    local["wo0"].wait()
    local["wo1"].wait()
    a_o = dot(ho, wo_o[0]).astype(BF16).astype(F32)
    a_p = dot(ho, wo_o[1]).astype(BF16).astype(F32)
    c_wo0.wait_recv()
    c_wo1.wait_recv()
    c_ho.wait_recv()
    hp = ho_p[...]
    a_o = a_o + dot(hp, wo_p[0]).astype(BF16).astype(F32)
    a_p = a_p + dot(hp, wo_p[1]).astype(BF16).astype(F32)
    after = (tok_f + a_o).astype(BF16).astype(F32)
    after_p = (tok_pf + a_p).astype(BF16).astype(F32)
    squares = jnp.sum(after * after, axis=1, keepdims=True) + jnp.sum(
        after_p * after_p, axis=1, keepdims=True
    )
    normed = (after * lax.rsqrt(squares / D + epsilon) * norm_ffn[...]).astype(BF16)

    chosen = dot(sel_m[:, :R].astype(BF16), normed).astype(BF16)
    xs[...] = chosen.astype(F32).reshape(EXPERTS, SLOT, H).astype(BF16)
    xz[0] = normed
    c_zr = {}
    for trip in TRIPS:
        for i in trip:
            if i:
                c_zr[i] = remote(xs.at[(z + i) % Z], zr.at[Z - i], zpeer[i])
    c_xz = {}
    for i in (1, 7, 2, 6, 3, 5, 4):
        c_xz[i] = remote(xz.at[0], xz.at[Z - i], zpeer[i])
    gate_row = gate_vec[...].astype(F32)
    gate_row = jnp.concatenate([gate_row[r : r + 1] for r in range(H // 128)], axis=1)
    logit = jnp.sum(normed.astype(F32) * gate_row, axis=1, keepdims=True)
    lg_s[...] = logit + jnp.zeros((R, 128), F32)
    c_lg = remote(lg_s, lg_r, partner)
    weights.two()
    weights.relay((0,))

    def new_state(h):
        cols = slice(h * hs, (h + 1) * hs)
        for s in range(R):
            ns[s, h] = decays[h] * st[s, h] + k_t[cols, s : s + 1] * v[s : s + 1, cols]

    new_state(0)

    chunks = [Gather(xe.at[c], 1 if c % 2 == 0 else -1) for c in range(len(TRIPS))]

    def pack(c):
        parts = []
        for i in TRIPS[c]:
            if i == 0:
                parts.append(xs[z].astype(F32))
            else:
                c_zr[Z - i].wait_recv()
                parts.append(zr[i].astype(F32))
        parts.append(jnp.zeros((32 - SLOT * len(parts), H), F32))
        rows = jnp.concatenate(parts, axis=0).astype(BF16)
        r, s = iota((R, 32), 0), iota((R, 32), 1)
        take = jnp.zeros((R, 32), F32)
        for j in range(len(TRIPS[c])):
            hit = (s - SLOT * j == r - CAP * j) & (r >= CAP * j) & (r < CAP * (j + 1))
            take = take + jnp.where(hit, 1.0, 0.0)
        xe[c, 0] = dot(take.astype(BF16), rows).astype(BF16)
        chunks[c].start()

    pack(0)
    weights.relay((3, 1))
    new_state(1)
    pack(1)
    chunks[0].one()
    pack(2)
    weights.relay((2,))

    for name in ("eg", "eu", "ed"):
        local[name].wait()
    for copy in (c_eg, c_eu, c_ed):
        copy.wait_recv()
    for t in range(2):
        for src, dst in ((eg, w1.at[0, t]), (eu, w1.at[1, t]), (ed, w2.at[t])):
            dst[:FE] = src[t]
            dst[FE:] = jnp.zeros((128 - FE, H), BF16)

    chunks[0].two()
    chunks[1].one()
    chunks[0].relay((0, 3))
    chunks[2].one()
    chunks[1].two()
    chunks[0].relay((1, 2))
    chunks[2].two()
    chunks[1].relay((0, 3, 1, 2))

    c_pe = {}

    def before_act(c):
        chunks[c].finish()
        x = jnp.concatenate([xe[c, place(p)] for p in range(PLANE)], axis=0)
        pre = dot_t(x, w1[...].reshape(4 * 128, H))
        pe_o[c] = pre
        pe_s[c] = pre.astype(BF16)
        c_pe[c] = remote(pe_s.at[c], pe_r.at[c], partner)

    def act(c):
        c_pe[c].wait_recv()
        pre = pe_o[c] + pe_r[c].astype(F32)
        hidden = (silu(pre[:, :256]) * pre[:, 256:]).astype(BF16)
        y = dot(hidden, w2[...].reshape(256, H))
        for p in range(PLANE):
            part = y[p * R : (p + 1) * R]
            y32[c, place(p)] = part
            yb[c, place(p)] = part.astype(BF16)
        at = yb.at
        low, high = lambda b: pl.ds(SIDE * b, 2), lambda b: pl.ds(SIDE * b + 2, 2)
        c_rb[c] = (
            remote(at[c, low(2)], rb.at[c, 0], second[1]),
            remote(at[c, high(2)], rb.at[c, 1], second[-1]),
        )
        c_rd[c] = (
            remote(at[c, high(1)], rd.at[c, 0], second[1]),
            remote(at[c, low(3)], rd.at[c, 1], second[-1]),
        )

    c_rb, c_rd, c_rf, c_ab, c_ad, c_af = {}, {}, {}, {}, {}, {}

    def sum_relay(c):
        c_rb[c][0].wait_recv()
        rs[c, 0] = (y32[c, SIDE : SIDE + 2] + rb[c, 0].astype(F32)).astype(BF16)
        up = remote(rs.at[c, 0], rf.at[c, 0], second[1])
        c_rb[c][1].wait_recv()
        rs[c, 1] = (y32[c, 3 * SIDE + 2 : 4 * SIDE] + rb[c, 1].astype(F32)).astype(BF16)
        c_rf[c] = (up, remote(rs.at[c, 1], rf.at[c, 1], second[-1]))

    def sum_second(c):
        via = chunks[c].via
        near, far = (1, 3) if via > 0 else (3, 1)
        c_rd[c][1].wait_recv()
        c_rf[c][0].wait_recv()
        low = y32[c, 0:2] + rf[c, 0].astype(F32) + rd[c, 1].astype(F32)
        c_rd[c][0].wait_recv()
        c_rf[c][1].wait_recv()
        high = y32[c, 2:4] + rf[c, 1].astype(F32) + rd[c, 0].astype(F32)
        total = (low[0], low[1], high[0], high[1])
        sb[c, 0] = total[2].astype(BF16)
        c_ab[c] = remote(sb.at[c, 0], ab.at[c], first[via])
        sb[c, 1] = total[far].astype(BF16)
        c_ad[c] = remote(sb.at[c, 1], ad.at[c], first[-via])
        sa[c, 0] = total[0]
        sa[c, 1] = total[near]

    def sum_two(c):
        c_ab[c].wait_recv()
        ax[c] = (sa[c, 1] + ab[c].astype(F32)).astype(BF16)
        c_af[c] = remote(ax.at[c], af.at[c], first[chunks[c].via])

    c_ret = {}

    def give_back(c):
        c_ad[c].wait_recv()
        c_af[c].wait_recv()
        total = (sa[c, 0] + ad[c].astype(F32) + af[c].astype(F32)).astype(BF16)
        n = len(TRIPS[c])
        s, r = iota((32, R), 0), iota((32, R), 1)
        put = jnp.zeros((32, R), F32)
        for j in range(n):
            hit = (s - SLOT * j == r - CAP * j) & (r >= CAP * j) & (r < CAP * (j + 1))
            put = put + jnp.where(hit, 1.0, 0.0)
        rows = dot(put.astype(BF16), total)
        for j, i in enumerate(TRIPS[c]):
            block = rows[j * SLOT : (j + 1) * SLOT].astype(BF16)
            if i == 0:
                zret[z] = block
            else:
                zs[i] = block
                c_ret[i] = remote(zs.at[i], zret.at[z], zpeer[i])

    before_act(0)
    chunks[2].relay((0, 3, 1, 2))
    before_act(1)
    act(0)
    weights.finish()
    before_act(2)
    act(1)
    sum_relay(0)

    for p in range(PLANE):
        for t, dst in enumerate((wdg, wdu, wdd)):
            dst[p, :FD] = wbuf[place(p), t]
            dst[p, FD:] = jnp.zeros((32 - FD, H), BF16)
    act(2)
    sum_second(0)
    sum_relay(1)
    for i in range(1, Z):
        c_xz[i].wait_recv()
    x = xz[...].reshape(Z * R, H)
    for t, w in enumerate((wdg, wdu)):
        pre = dot_t(x, w[...].reshape(PLANE * 32, H))
        pd_o[t] = pre
        pd_s[t] = pre.astype(BF16)
    c_pd = remote(pd_s, pd_r, partner)
    sum_two(0)
    sum_second(1)
    sum_relay(2)
    c_pd.wait_recv()
    gate = pd_o[0] + pd_r[0].astype(F32)
    up = pd_o[1] + pd_r[1].astype(F32)
    y = dot((silu(gate) * up).astype(BF16), wdd[...].reshape(PLANE * 32, H))
    yz0[...] = y[:R]
    yzs[...] = y.astype(BF16).reshape(Z, R, H)
    give_back(0)
    c_yz = {}
    for i in range(1, Z):
        c_yz[i] = remote(yzs.at[i], yzr.at[Z - i], zpeer[i])
    sum_two(1)
    sum_second(2)
    give_back(1)
    sum_two(2)
    give_back(2)

    c_lg.wait_recv()
    open_ = 1.0 / (1.0 + jnp.exp(-(lg_s[:, :1] + lg_r[:, :1])))
    dense = yz0[...]
    for i in range(1, Z):
        c_yz[i].wait_recv()
        dense = dense + yzr[Z - i].astype(F32)
    for i in range(1, Z):
        c_ret[i].wait_recv()
    back = zret[...].astype(F32).reshape(EXPERTS * SLOT, H).astype(BF16)
    moe = dot(comb_m[:, : EXPERTS * SLOT].astype(BF16), back)
    mixed[...] = (after + moe + open_ * dense).astype(BF16)
    for copy in sent:
        copy.wait_send()


def store(a_in, b_in, a_out, b_out, sems):
    first = pltpu.make_async_copy(b_in, b_out, sems.at[0])
    second = pltpu.make_async_copy(a_in, a_out, sems.at[1])
    first.start()
    second.start()
    first.wait()
    second.wait()


def body(
    tokens,
    state,
    norm_mix,
    w_query,
    w_key,
    w_value,
    w_out,
    norm_ffn,
    gate_vector,
    dense_gate,
    dense_up,
    dense_down,
    exp_gate,
    exp_up,
    exp_down,
    routes,
    route_w,
):
    R, H = tokens.shape
    heads, hs = state.shape[1], state.shape[2]
    HW = heads * hs
    FE = exp_gate.shape[2]
    FD = dense_gate.shape[1]
    Z, C = EXPERTS, len(TRIPS)
    vm = pl.BlockSpec(memory_space=pltpu.VMEM)
    hbm = pl.BlockSpec(memory_space=pltpu.HBM)
    V = pltpu.VMEM
    sem = lambda *shape: pltpu.SemaphoreType.DMA(shape)
    operands = (
        tokens,
        norm_mix.reshape(1, -1),
        routes.T,
        route_w.T,
        norm_ffn.reshape(1, -1),
        gate_vector.reshape(-1, 128),
        state,
        w_query,
        w_key,
        w_value,
        w_out,
        dense_gate.T,
        dense_up.T,
        dense_down,
        exp_gate[0].T,
        exp_up[0].T,
        exp_down,
    )
    held = [pltpu.with_memory_space_constraint(x, pltpu.HBM) for x in operands]
    mixed, new_state = pl.pallas_call(
        kernel,
        out_shape=(pltpu.VMEM((R, H), BF16), pltpu.VMEM(state.shape, F32)),
        in_specs=[hbm] * 17,
        out_specs=(vm, vm),
        scratch_shapes=[
            V((R, H), BF16),
            V((1, 2 * H), F32),
            V((routes.shape[1], R), jnp.int32),
            V((routes.shape[1], R), BF16),
            V((1, H), F32),
            V((H // 128, 128), BF16),
            V((R, H), BF16),
            V((2, H, HW), BF16),
            V((2, H, HW), BF16),
            V((2, H, HW), BF16),
            V((2, HW, H), BF16),
            V((2, HW, H), BF16),
            V((2, FE, H), BF16),
            V((2, FE, H), BF16),
            V((2, FE, H), BF16),
            V(state.shape, F32),
            V((R, HW), BF16),
            V((R, HW), BF16),
            V((EXPERTS * SLOT, 128), F32),
            V((R, 128), F32),
            V((R, 128), F32),
            V((R, 128), F32),
            V((PLANE, 3, FD, H), BF16),
            V((PLANE, 32, H), BF16),
            V((PLANE, 32, H), BF16),
            V((PLANE, 32, H), BF16),
            V((2, 2, 128, H), BF16),
            V((2, 128, H), BF16),
            V((EXPERTS, SLOT, H), BF16),
            V((Z, SLOT, H), BF16),
            V((Z, R, H), BF16),
            V((C, PLANE, R, H), BF16),
            V((C, PLANE * R, 512), F32),
            V((C, PLANE * R, 512), BF16),
            V((C, PLANE * R, 512), BF16),
            V((2, Z * R, PLANE * 32), F32),
            V((2, Z * R, PLANE * 32), BF16),
            V((2, Z * R, PLANE * 32), BF16),
            V((C, PLANE, R, H), F32),
            V((C, PLANE, R, H), BF16),
            V((C, 2, 2, R, H), BF16),
            V((C, 2, 2, R, H), BF16),
            V((C, 2, 2, R, H), BF16),
            V((C, 2, 2, R, H), BF16),
            V((C, 2, R, H), F32),
            V((C, 2, R, H), BF16),
            V((C, R, H), BF16),
            V((C, R, H), BF16),
            V((C, R, H), BF16),
            V((C, R, H), BF16),
            V((Z, SLOT, H), BF16),
            V((EXPERTS, SLOT, H), BF16),
            V((R, H), F32),
            V((Z, R, H), BF16),
            V((Z, R, H), BF16),
            sem(32),
            sem(160),
            sem(160),
        ],
        compiler_params=pltpu.CompilerParams(
            collective_id=0, has_side_effects=True, vmem_limit_bytes=50 * 1024 * 1024
        ),
        name="layer",
    )(
        *held
    )
    return pl.pallas_call(
        store,
        out_shape=(
            jax.ShapeDtypeStruct((R, H), BF16),
            jax.ShapeDtypeStruct(state.shape, F32),
        ),
        in_specs=[vm, vm],
        out_specs=(hbm, hbm),
        scratch_shapes=[sem(2)],
        name="store",
    )(
        pltpu.with_memory_space_constraint(mixed, pltpu.VMEM),
        pltpu.with_memory_space_constraint(new_state, pltpu.VMEM),
    )


def solution(mesh):
    return jax.shard_map(
        body,
        mesh=mesh,
        in_specs=(
            P("ep", "tp"),
            P("ep", "tp", None, None),
            P(),
            P(None, "tp"),
            P(None, "tp"),
            P(None, "tp"),
            P("tp", None),
            P("tp"),
            P("tp"),
            P("tp", "ep"),
            P("tp", "ep"),
            P("ep", "tp"),
            P("ep", None, "tp"),
            P("ep", None, "tp"),
            P("ep", "tp", None),
            P("ep", None),
            P("ep", None),
        ),
        out_specs=(P("ep", "tp"), P("ep", "tp", None, None)),
        check_vma=False,
    )
```

time: 136 us -> 70.2 us (0.52)
  the two profiles are of different devices: /device:TPU:1 before, /device:TPU:2 now
where the time goes in v1:
time: 70.2 us; the launch traced here: 70.1 us
  Pallas kernels  69.4 us (99%)
    pallas_call x1, Pallas kernels, body(): pl.pallas_call(kernel, out_shape=(pltpu.VMEM((R, H), BF16), pltpu.VMEM(st...  68.1 us

profile of v1, /device:TPU:2, one launch (start us, length us, event | category | flops | bytes accessed | tf_op | source)
XLA Modules:
  0.0 70.1 jit_solution(11018681936875892901)
XLA Ops:
  0.6 68.1 %layer.1 = (bf16[16,1024]{1,0:T(8,128)(2,1)S(1)}, f32[16,2,128,128]{3,2,1,0:T(8,128)S(1)}) custom-call(bf16[16,1024]{1,0:T(8,128)(2,1)} %tokens_h.1, f32[1,2048]{1,0:T(1,128)} %bitcast.17, s32[2,16]{1,0:T(2,128)} %bitcast.20, bf16[2,16]{1,0:T(2,128)(2,1)} %bitcast.21, f32[1,1024]{1,0:T(1,128)} %bitcast.18, bf16[8,128]{1,0:T(8,128)(2,1)} %bitcast.19, ...), custom_call_target="tpu_custom_call" | custom-call | tf_op jit(solution)/shard_map/layer/pallas_call | solution.py:614
  68.7 1.3 %store.1 = (bf16[16,1024]{1,0:T(8,128)(2,1)}, f32[16,2,128,128]{3,2,1,0:T(8,128)}) custom-call(bf16[16,1024]{1,0:T(8,128)(2,1)S(1)} %get-tuple-element.4.a_in, f32[16,2,128,128]{3,2,1,0:T(8,128)S(1)} %get-tuple-element.5.b_in), custom_call_target="tpu_custom_call" | custom-call | tf_op jit(solution)/shard_map/store/pallas_call | solution.py:686

commit v2 on v1

--- a/solution.py
+++ b/solution.py
@@ -12,7 +12,7 @@
 SLOT = 8
 SIDE = 4
 PLANE = SIDE * SIDE
-TRIPS = ((0, 1, 7), (2, 6, 3), (5, 4))
+TRIPS = ((0, 1, 7), (3, 5, 4), (2, 6))
 epsilon = 1e-06
 MESH = pl.DeviceIdType.MESH
 F32 = jnp.float32
@@ -239,6 +239,20 @@
     load("eu", exp_up.at[:, own], eu.at[tp])
     load("ed", exp_down.at[0, :, own], ed.at[tp])
 
+    local["s0"].wait()
+    pl.semaphore_wait(barrier, len(greeted))
+
+    c_tok = remote(tokens, tok_p, partner)
+    weights = Gather(wbuf, 1)
+    for t in range(3):
+        local[f"d{t}"].wait()
+    weights.start()
+    c_wo0 = remote(w_out.at[:, oth], wo_p.at[0], partner)
+    c_wo1 = remote(w_out.at[:, own], wo_p.at[1], partner)
+    c_eg = remote(exp_gate.at[:, oth], eg.at[tp], partner)
+    c_eu = remote(exp_up.at[:, oth], eu.at[tp], partner)
+    c_ed = remote(exp_down.at[0, :, oth], ed.at[tp], partner)
+
     for t in (2, 3):
         local[f"s{t}"].wait()
     row_id = iota((EXPERTS, R), 0)
@@ -264,21 +278,8 @@
     sel_m[...] = jnp.concatenate(picks, axis=0)
     scaled.append(jnp.zeros((128 - EXPERTS * SLOT, 128), F32))
     comb_m[...] = jnp.concatenate(scaled, axis=0).T[:R]
-
-    for t in (0, 1, 4, 5):
+    for t in (1, 4, 5):
         local[f"s{t}"].wait()
-    for t in range(3):
-        local[f"d{t}"].wait()
-    pl.semaphore_wait(barrier, len(greeted))
-
-    c_tok = remote(tokens, tok_p, partner)
-    weights = Gather(wbuf, 1)
-    weights.start()
-    c_wo0 = remote(w_out.at[:, oth], wo_p.at[0], partner)
-    c_wo1 = remote(w_out.at[:, own], wo_p.at[1], partner)
-    c_eg = remote(exp_gate.at[:, oth], eg.at[tp], partner)
-    c_eu = remote(exp_up.at[:, oth], eu.at[tp], partner)
-    c_ed = remote(exp_down.at[0, :, oth], ed.at[tp], partner)
 
     tok_f = tokens[...].astype(F32)
     c_tok.wait_recv()
@@ -321,12 +322,12 @@
         spread = jnp.mean(dev * dev, axis=1, keepdims=True)
         ho_o[:, cols] = (dev * lax.rsqrt(spread + epsilon)).astype(BF16)
     c_ho = remote(ho_o, ho_p, partner)
-    weights.one()
     ho = ho_o[...]
     local["wo0"].wait()
     local["wo1"].wait()
     a_o = dot(ho, wo_o[0]).astype(BF16).astype(F32)
     a_p = dot(ho, wo_o[1]).astype(BF16).astype(F32)
+    weights.one()
     c_wo0.wait_recv()
     c_wo1.wait_recv()
     c_ho.wait_recv()
@@ -344,10 +345,8 @@
     xs[...] = chosen.astype(F32).reshape(EXPERTS, SLOT, H).astype(BF16)
     xz[0] = normed
     c_zr = {}
-    for trip in TRIPS:
-        for i in trip:
-            if i:
-                c_zr[i] = remote(xs.at[(z + i) % Z], zr.at[Z - i], zpeer[i])
+    for i in (1, 7, 4, 3, 5, 2, 6):
+        c_zr[i] = remote(xs.at[(z + i) % Z], zr.at[Z - i], zpeer[i])
     c_xz = {}
     for i in (1, 7, 2, 6, 3, 5, 4):
         c_xz[i] = remote(xz.at[0], xz.at[Z - i], zpeer[i])
@@ -356,7 +355,6 @@
     logit = jnp.sum(normed.astype(F32) * gate_row, axis=1, keepdims=True)
     lg_s[...] = logit + jnp.zeros((R, 128), F32)
     c_lg = remote(lg_s, lg_r, partner)
-    weights.two()
     weights.relay((0,))
 
     def new_state(h):
@@ -365,6 +363,16 @@
             ns[s, h] = decays[h] * st[s, h] + k_t[cols, s : s + 1] * v[s : s + 1, cols]
 
     new_state(0)
+
+    for name in ("eg", "eu", "ed"):
+        local[name].wait()
+    for copy in (c_eg, c_eu, c_ed):
+        copy.wait_recv()
+    for t in range(2):
+        for src, dst in ((eg, w1.at[0, t]), (eu, w1.at[1, t]), (ed, w2.at[t])):
+            dst[:FE] = src[t]
+            dst[FE:] = jnp.zeros((128 - FE, H), BF16)
+    new_state(1)
 
     chunks = [Gather(xe.at[c], 1 if c % 2 == 0 else -1) for c in range(len(TRIPS))]
 
@@ -387,69 +395,63 @@
         chunks[c].start()
 
     pack(0)
+    weights.two()
+    pack(2)
+    pack(1)
     weights.relay((3, 1))
-    new_state(1)
-    pack(1)
     chunks[0].one()
-    pack(2)
+    chunks[0].relay((0,))
+    chunks[2].one()
     weights.relay((2,))
-
-    for name in ("eg", "eu", "ed"):
-        local[name].wait()
-    for copy in (c_eg, c_eu, c_ed):
-        copy.wait_recv()
-    for t in range(2):
-        for src, dst in ((eg, w1.at[0, t]), (eu, w1.at[1, t]), (ed, w2.at[t])):
-            dst[:FE] = src[t]
-            dst[FE:] = jnp.zeros((128 - FE, H), BF16)
-
     chunks[0].two()
+    chunks[2].relay((0,))
     chunks[1].one()
-    chunks[0].relay((0, 3))
-    chunks[2].one()
+    chunks[0].relay((3, 1))
+    chunks[1].relay((0,))
+    chunks[2].two()
+    chunks[2].relay((3, 1))
+    chunks[0].relay((2,))
     chunks[1].two()
-    chunks[0].relay((1, 2))
-    chunks[2].two()
-    chunks[1].relay((0, 3, 1, 2))
 
     c_pe = {}
 
     def before_act(c):
         chunks[c].finish()
-        x = jnp.concatenate([xe[c, place(p)] for p in range(PLANE)], axis=0)
-        pre = dot_t(x, w1[...].reshape(4 * 128, H))
+        pre = dot_t(xe[c].reshape(PLANE * R, H), w1[...].reshape(4 * 128, H))
         pe_o[c] = pre
-        pe_s[c] = pre.astype(BF16)
+        for b in range(SIDE):
+            for a in range(SIDE):
+                f = SIDE * b + a
+                pe_s[c, SIDE * a + b] = pre[f * R : (f + 1) * R].astype(BF16)
         c_pe[c] = remote(pe_s.at[c], pe_r.at[c], partner)
 
     def act(c):
         c_pe[c].wait_recv()
-        pre = pe_o[c] + pe_r[c].astype(F32)
+        pre = pe_o[c] + pe_r[c].reshape(PLANE * R, 512).astype(F32)
         hidden = (silu(pre[:, :256]) * pre[:, 256:]).astype(BF16)
-        y = dot(hidden, w2[...].reshape(256, H))
-        for p in range(PLANE):
-            part = y[p * R : (p + 1) * R]
-            y32[c, place(p)] = part
-            yb[c, place(p)] = part.astype(BF16)
+        down = w2[...].reshape(256, H)
+        yb[c] = dot(hidden[6 * R : 14 * R], down).astype(BF16).reshape(8, R, H)
         at = yb.at
-        low, high = lambda b: pl.ds(SIDE * b, 2), lambda b: pl.ds(SIDE * b + 2, 2)
         c_rb[c] = (
-            remote(at[c, low(2)], rb.at[c, 0], second[1]),
-            remote(at[c, high(2)], rb.at[c, 1], second[-1]),
+            remote(at[c, pl.ds(2, 2)], rb.at[c, 0], second[1]),
+            remote(at[c, pl.ds(4, 2)], rb.at[c, 1], second[-1]),
         )
         c_rd[c] = (
-            remote(at[c, high(1)], rd.at[c, 0], second[1]),
-            remote(at[c, low(3)], rd.at[c, 1], second[-1]),
+            remote(at[c, pl.ds(0, 2)], rd.at[c, 0], second[1]),
+            remote(at[c, pl.ds(6, 2)], rd.at[c, 1], second[-1]),
         )
+        y32[c, 4:6] = dot(hidden[4 * R : 6 * R], down).reshape(2, R, H)
+        y32[c, 6:8] = dot(hidden[14 * R :], down).reshape(2, R, H)
+        y32[c, 0:4] = dot(hidden[: 4 * R], down).reshape(4, R, H)
 
     c_rb, c_rd, c_rf, c_ab, c_ad, c_af = {}, {}, {}, {}, {}, {}
 
     def sum_relay(c):
         c_rb[c][0].wait_recv()
-        rs[c, 0] = (y32[c, SIDE : SIDE + 2] + rb[c, 0].astype(F32)).astype(BF16)
+        rs[c, 0] = (y32[c, 4:6] + rb[c, 0].astype(F32)).astype(BF16)
         up = remote(rs.at[c, 0], rf.at[c, 0], second[1])
         c_rb[c][1].wait_recv()
-        rs[c, 1] = (y32[c, 3 * SIDE + 2 : 4 * SIDE] + rb[c, 1].astype(F32)).astype(BF16)
+        rs[c, 1] = (y32[c, 6:8] + rb[c, 1].astype(F32)).astype(BF16)
         c_rf[c] = (up, remote(rs.at[c, 1], rf.at[c, 1], second[-1]))
 
     def sum_second(c):
@@ -495,47 +497,54 @@
                 zs[i] = block
                 c_ret[i] = remote(zs.at[i], zret.at[z], zpeer[i])
 
-    before_act(0)
-    chunks[2].relay((0, 3, 1, 2))
-    before_act(1)
-    act(0)
     weights.finish()
-    before_act(2)
-    act(1)
-    sum_relay(0)
 
     for p in range(PLANE):
         for t, dst in enumerate((wdg, wdu, wdd)):
             dst[p, :FD] = wbuf[place(p), t]
             dst[p, FD:] = jnp.zeros((32 - FD, H), BF16)
+
+    def dense_before():
+        for i in range(1, Z):
+            c_xz[i].wait_recv()
+        x = xz[...].reshape(Z * R, H)
+        for t, w in enumerate((wdg, wdu)):
+            pre = dot_t(x, w[...].reshape(PLANE * 32, H))
+            pd_o[t] = pre
+            pd_s[t] = pre.astype(BF16)
+        return remote(pd_s, pd_r, partner)
+
+    def dense_act():
+        gate = pd_o[0] + pd_r[0].astype(F32)
+        up = pd_o[1] + pd_r[1].astype(F32)
+        y = dot((silu(gate) * up).astype(BF16), wdd[...].reshape(PLANE * 32, H))
+        yz0[...] = y[:R]
+        yzs[...] = y.astype(BF16).reshape(Z, R, H)
+        return {i: remote(yzs.at[i], yzr.at[Z - i], zpeer[i]) for i in (4, 3, 5, 2, 6, 1, 7)}
+
+    chunks[1].relay((3, 1))
+    chunks[2].relay((2,))
+    before_act(0)
+    c_pd = dense_before()
+    chunks[1].relay((2,))
+    before_act(2)
+    act(0)
+    before_act(1)
+    c_pd.wait_recv()
+    c_yz = dense_act()
+    act(1)
+    sum_relay(0)
     act(2)
+    sum_relay(1)
     sum_second(0)
-    sum_relay(1)
-    for i in range(1, Z):
-        c_xz[i].wait_recv()
-    x = xz[...].reshape(Z * R, H)
-    for t, w in enumerate((wdg, wdu)):
-        pre = dot_t(x, w[...].reshape(PLANE * 32, H))
-        pd_o[t] = pre
-        pd_s[t] = pre.astype(BF16)
-    c_pd = remote(pd_s, pd_r, partner)
+    sum_relay(2)
+    sum_second(1)
     sum_two(0)
-    sum_second(1)
-    sum_relay(2)
-    c_pd.wait_recv()
-    gate = pd_o[0] + pd_r[0].astype(F32)
-    up = pd_o[1] + pd_r[1].astype(F32)
-    y = dot((silu(gate) * up).astype(BF16), wdd[...].reshape(PLANE * 32, H))
-    yz0[...] = y[:R]
-    yzs[...] = y.astype(BF16).reshape(Z, R, H)
+    sum_second(2)
+    sum_two(1)
     give_back(0)
-    c_yz = {}
-    for i in range(1, Z):
-        c_yz[i] = remote(yzs.at[i], yzr.at[Z - i], zpeer[i])
-    sum_two(1)
-    sum_second(2)
+    sum_two(2)
     give_back(1)
-    sum_two(2)
     give_back(2)
 
     c_lg.wait_recv()
@@ -650,13 +659,13 @@
             V((Z, R, H), BF16),
             V((C, PLANE, R, H), BF16),
             V((C, PLANE * R, 512), F32),
-            V((C, PLANE * R, 512), BF16),
-            V((C, PLANE * R, 512), BF16),
+            V((C, PLANE, R, 512), BF16),
+            V((C, PLANE, R, 512), BF16),
             V((2, Z * R, PLANE * 32), F32),
             V((2, Z * R, PLANE * 32), BF16),
             V((2, Z * R, PLANE * 32), BF16),
-            V((C, PLANE, R, H), F32),
-            V((C, PLANE, R, H), BF16),
+            V((C, 8, R, H), F32),
+            V((C, 8, R, H), BF16),
             V((C, 2, 2, R, H), BF16),
             V((C, 2, 2, R, H), BF16),
             V((C, 2, 2, R, H), BF16),

time: 70.2 us -> 63.7 us (0.907)
  the two profiles are of different devices: /device:TPU:2 before, /device:TPU:1 now
where the time goes in v2:
time: 63.7 us; the launch traced here: 62.8 us
  Pallas kernels  62.1 us (97%)
  between operations  0.65 us (1%)
    pallas_call x1, Pallas kernels, body(): pl.pallas_call(kernel, out_shape=(pltpu.VMEM((R, H), BF16), pltpu.VMEM(st...  60.8 us
    pallas_call x1, Pallas kernels, body(): pl.pallas_call(store, out_shape=(jax.ShapeDtypeStruct((R, H), BF16), jax....  1.34 us

profile of v2, /device:TPU:1, one launch (start us, length us, event | category | flops | bytes accessed | tf_op | source)
XLA Modules:
  0.0 62.8 jit_solution(528445195672155888)
XLA Ops:
  0.6 60.8 %layer.1 = (bf16[16,1024]{1,0:T(8,128)(2,1)S(1)}, f32[16,2,128,128]{3,2,1,0:T(8,128)S(1)}) custom-call(bf16[16,1024]{1,0:T(8,128)(2,1)} %tokens_h.1, f32[1,2048]{1,0:T(1,128)} %bitcast.17, s32[2,16]{1,0:T(2,128)} %bitcast.20, bf16[2,16]{1,0:T(2,128)(2,1)} %bitcast.21, f32[1,1024]{1,0:T(1,128)} %bitcast.18, bf16[8,128]{1,0:T(8,128)(2,1)} %bitcast.19, ...), custom_call_target="tpu_custom_call" | custom-call | tf_op jit(solution)/shard_map/layer/pallas_call | solution.py:623
  61.4 1.3 %store.1 = (bf16[16,1024]{1,0:T(8,128)(2,1)}, f32[16,2,128,128]{3,2,1,0:T(8,128)}) custom-call(bf16[16,1024]{1,0:T(8,128)(2,1)S(1)} %get-tuple-element.4.a_in, f32[16,2,128,128]{3,2,1,0:T(8,128)S(1)} %get-tuple-element.5.b_in), custom_call_target="tpu_custom_call" | custom-call | tf_op jit(solution)/shard_map/store/pallas_call | solution.py:695

commit v3 on v2

v3 whole, which is shorter than its diff:
```python
import functools

import jax
import jax.numpy as jnp
from jax import lax
from jax.experimental import pallas as pl
from jax.experimental.pallas import tpu as pltpu
from jax.sharding import PartitionSpec as P

EXPERTS = 8
CAP = 5
SLOT = 8
SIDE = 4
PLANE = SIDE * SIDE
NEAR = (0, 1, 7, 2, 6, 3, 5, 4)
PACKED = (4, 3, 5, 2, 6, 1, 7, 0)
CHUNKS = (24, 16, 16)
GROUPS = 32
LOADS = 21
epsilon = 1e-06
MESH = pl.DeviceIdType.MESH
F32 = jnp.float32
BF16 = jnp.bfloat16


def dot(a, b):
    return jnp.dot(a, b, preferred_element_type=F32)


def dot_t(a, b):
    return lax.dot_general(a, b, (((1,), (1,)), ((), ())), preferred_element_type=F32)


def silu(v):
    return v / (1.0 + jnp.exp(-v))


def iota(shape, dim):
    return lax.broadcasted_iota(jnp.int32, shape, dim)


def kernel(
    tokens_h,
    norm_mix_h,
    routes_h,
    route_w_h,
    norm_ffn_h,
    gate_vec_h,
    state,
    w_query,
    w_key,
    w_value,
    w_out,
    dense_gate,
    dense_up,
    dense_down,
    exp_gate,
    exp_up,
    exp_down,
    mixed,
    ns,
    tokens,
    norm_mix,
    routes,
    route_w,
    norm_ffn,
    gate_vec,
    tok_p,
    wq,
    wk,
    wv,
    wo_o,
    wo_p,
    eg,
    eu,
    ed,
    st,
    ho_o,
    ho_p,
    sel_m,
    scl_m,
    lg_s,
    lg_r,
    wbuf,
    w1,
    w2,
    w1d,
    w2d,
    xs,
    zr,
    xe_a,
    xe_b,
    xe_d,
    pe_o_a,
    pe_o_b,
    pe_o_d,
    pe_s_a,
    pe_s_b,
    pe_s_d,
    pe_r_a,
    pe_r_b,
    pe_r_d,
    y_a,
    y_b,
    y_d,
    yb_a,
    yb_b,
    yb_d,
    rb_a,
    rb_b,
    rb_d,
    sb_a,
    sb_b,
    sb_d,
    ra_a,
    ra_b,
    ra_d,
    tot,
    zs,
    zret,
    lsem,
    ssem,
    rsem,
):
    R, H = tokens.shape
    D = 2 * H
    heads, hs = state.shape[1], state.shape[2]
    HW = heads * hs
    FE = eg.shape[1]
    FD = wbuf.shape[2]
    Z = EXPERTS
    me = lax.axis_index("ep")
    tp = lax.axis_index("tp")
    other = 1 - tp
    z, y_at, x_at = me // PLANE, (me // SIDE) % SIDE, me % SIDE

    def in_plane(dy, dx):
        return {
            "ep": z * PLANE + ((y_at + dy + SIDE) % SIDE) * SIDE + (x_at + dx + SIDE) % SIDE,
            "tp": tp,
        }

    first = {d: in_plane(tp * d, other * d) for d in (1, -1, 2)}
    second = {d: in_plane(other * d, tp * d) for d in (1, -1, 2)}
    zpeer = [{"ep": ((z + i) % Z) * PLANE + me % PLANE, "tp": tp} for i in range(Z)]
    partner = {"ep": me, "tp": other}

    own = pl.ds(pl.multiple_of(tp * H, H), H)
    oth = pl.ds(pl.multiple_of(other * H, H), H)

    sent = []

    class Group:
        def __init__(self, whole):
            self.k, self.whole = len(sent), whole
            sent.append(self)

        def copy(self, src, dst, dev):
            self.dev = dev
            return pltpu.make_async_remote_copy(
                src_ref=src,
                dst_ref=dst,
                send_sem=ssem.at[self.k],
                recv_sem=rsem.at[self.k],
                device_id=dev,
                device_id_type=MESH,
            )

        def add(self, src, dst, dev):
            self.copy(src, dst, dev).start()

        def wait_recv(self):
            self.copy(self.whole, self.whole, self.dev).wait_recv()

        def wait_send(self):
            self.copy(self.whole, self.whole, self.dev).wait_send()

    def remote(src, dst, dev):
        group = Group(dst)
        group.add(src, dst, dev)
        return group

    local = {}

    def load(name, src, dst):
        copy = pltpu.make_async_copy(src, dst, lsem.at[len(local)])
        copy.start()
        local[name] = copy

    HOPS = ((1, 1), (-1, 2), (2, 3))
    BACK = ((2, 3), (-1, 1), (1, 2))

    class Gather:
        def __init__(self, buf):
            self.at = buf.at

        def spread(self, *todo):
            for d, b in HOPS:
                for a in todo:
                    self.across.add(self.at[a], self.at[SIDE * b + a], second[d])

        def start(self):
            at = self.at
            self.near, self.far = Group(at[pl.ds(1, 2)]), Group(at[3])
            self.across = Group(at[pl.ds(SIDE, 3 * SIDE)])
            self.near.add(at[0], at[1], first[1])
            self.near.add(at[0], at[2], first[-1])
            self.far.add(at[0], at[3], first[2])
            self.spread(0)

        def go(self):
            self.near.wait_recv()
            self.spread(1, 2)
            self.far.wait_recv()
            self.spread(3)

    class Ring:
        def __init__(self, buf):
            self.at, self.step = buf.at, 0

        def start(self):
            at, t = self.at, self.step
            if t:
                self.group.wait_recv()
            up, down = max(0, 2 * t), max(0, 2 * t - 1)
            if t < 3:
                self.group = Group(at[pl.ds(2 * t + 1, 2)])
                self.group.add(at[up], at[2 * t + 2], zpeer[1])
                self.group.add(at[down], at[2 * t + 1], zpeer[-1])
            elif t == 3:
                self.group = Group(at[7])
                self.group.add(at[up, pl.ds(0, 2)], at[7, pl.ds(0, 2)], zpeer[1])
                self.group.add(at[down, pl.ds(2, 1)], at[7, pl.ds(2, 1)], zpeer[-1])
            self.step = t + 1

    small = (
        (tokens_h, tokens),
        (norm_mix_h, norm_mix),
        (routes_h, routes),
        (route_w_h, route_w),
        (norm_ffn_h, norm_ffn),
        (gate_vec_h, gate_vec),
    )
    barrier = pltpu.get_barrier_semaphore()
    greeted = [partner, *first.values(), *second.values()] + zpeer[1:]
    for dev in greeted:
        pl.semaphore_signal(barrier, inc=1, device_id=dev, device_id_type=MESH)

    for t, (src, dst) in enumerate(small):
        load(f"s{t}", src, dst)
    for t, src in enumerate((dense_gate, dense_up, dense_down)):
        load(f"d{t}", src, wbuf.at[0, t])
    for t, (src, dst) in enumerate(((w_query, wq), (w_key, wk), (w_value, wv))):
        load(f"p{t}o", src.at[own, :], dst.at[0])
        load(f"p{t}p", src.at[oth, :], dst.at[1])
    load("st", state, st)
    load("wo0", w_out.at[:, own], wo_o.at[0])
    load("wo1", w_out.at[:, oth], wo_o.at[1])
    load("eg", exp_gate.at[:, own], eg.at[tp])
    load("eu", exp_up.at[:, own], eu.at[tp])
    load("ed", exp_down.at[0, :, own], ed.at[tp])

    local["s0"].wait()
    pl.semaphore_wait(barrier, len(greeted))

    c_tok = remote(tokens, tok_p, partner)
    weights = Ring(wbuf)
    for t in range(3):
        local[f"d{t}"].wait()
    weights.start()
    c_wo = Group(wo_p)
    c_wo.add(w_out.at[:, oth], wo_p.at[0], partner)
    c_wo.add(w_out.at[:, own], wo_p.at[1], partner)
    c_eg = remote(exp_gate.at[:, oth], eg.at[tp], partner)
    c_eu = remote(exp_up.at[:, oth], eu.at[tp], partner)
    c_ed = remote(exp_down.at[0, :, oth], ed.at[tp], partner)

    for t in (2, 3):
        local[f"s{t}"].wait()
    row_id = iota((EXPERTS, R), 0)
    wt = jnp.zeros((EXPERTS, R), F32)
    member = jnp.zeros((EXPERTS, R), F32)
    named = routes[...]
    gains = route_w[...].astype(F32)
    for t in range(routes.shape[0]):
        hit = row_id == named[t : t + 1, :]
        wt = wt + jnp.where(hit, gains[t : t + 1, :], 0.0)
        member = member + jnp.where(hit, 1.0, 0.0)
    blank = jnp.zeros((EXPERTS, 128 - R), F32)
    wt = jnp.concatenate([wt, blank], axis=1)
    member = jnp.concatenate([member, blank], axis=1)
    before = jnp.where(iota((128, 128), 0) < iota((128, 128), 1), 1.0, 0.0).astype(BF16)
    rank = dot(member.astype(BF16), before)
    slot_id = iota((SLOT, 128), 0).astype(F32)
    picks = []
    for e in range(EXPERTS):
        pick = jnp.where(rank[e : e + 1] == slot_id, member[e : e + 1], 0.0)
        picks.append(pick)
        scl_m[e] = pick * wt[e : e + 1]
    sel_m[...] = jnp.concatenate(picks, axis=0)
    for t in (1, 4, 5):
        local[f"s{t}"].wait()

    tok_f = tokens[...].astype(F32)
    c_tok.wait_recv()
    tok_pf = tok_p[...].astype(F32)
    total = jnp.sum(tok_f * tok_f, axis=1, keepdims=True) + jnp.sum(
        tok_pf * tok_pf, axis=1, keepdims=True
    )
    scale = lax.rsqrt(total / D + epsilon)
    gain_o = norm_mix[:, own]
    gain_p = norm_mix[:, oth]
    nx_o = (tok_f * scale * gain_o).astype(BF16)
    nx_p = (tok_pf * scale * gain_p).astype(BF16)
    proj = []
    for t, w in enumerate((wq, wk, wv)):
        local[f"p{t}o"].wait()
        part = dot(nx_o, w[0])
        local[f"p{t}p"].wait()
        proj.append((part + dot(nx_p, w[1])).astype(BF16).astype(F32))
    q, k, v = proj
    k = k * hs ** (-0.5)
    pad = jnp.zeros((128 - R, HW), F32)
    q_t = jnp.concatenate([q, pad], axis=0).T
    k_t = jnp.concatenate([k, pad], axis=0).T
    head_id = tp * heads
    local["st"].wait()
    decays = []
    for h in range(heads):
        cols = slice(h * hs, (h + 1) * hs)
        idv = jnp.zeros((1, 128), F32) + (head_id + h).astype(F32)
        decay = 1.0 - jnp.exp2(-3.0 - 2.0 * idv)
        decays.append(decay)
        rows = []
        for s in range(R):
            rows.append(jnp.sum(st[s, h] * q_t[cols, s : s + 1], axis=0, keepdims=True))
        qs = jnp.concatenate(rows, axis=0)
        qk = jnp.sum(q[:, cols] * k[:, cols], axis=1, keepdims=True)
        read = decay * qs + qk * v[:, cols]
        centre = jnp.mean(read, axis=1, keepdims=True)
        dev = read - centre
        spread = jnp.mean(dev * dev, axis=1, keepdims=True)
        ho_o[:, cols] = (dev * lax.rsqrt(spread + epsilon)).astype(BF16)
    c_ho = remote(ho_o, ho_p, partner)
    ho = ho_o[...]
    local["wo0"].wait()
    local["wo1"].wait()
    a_o = dot(ho, wo_o[0]).astype(BF16).astype(F32)
    a_p = dot(ho, wo_o[1]).astype(BF16).astype(F32)
    c_wo.wait_recv()
    c_ho.wait_recv()
    hp = ho_p[...]
    a_o = a_o + dot(hp, wo_p[0]).astype(BF16).astype(F32)
    a_p = a_p + dot(hp, wo_p[1]).astype(BF16).astype(F32)
    after = (tok_f + a_o).astype(BF16).astype(F32)
    after_p = (tok_pf + a_p).astype(BF16).astype(F32)
    squares = jnp.sum(after * after, axis=1, keepdims=True) + jnp.sum(
        after_p * after_p, axis=1, keepdims=True
    )
    normed = (after * lax.rsqrt(squares / D + epsilon) * norm_ffn[...]).astype(BF16)

    chosen = dot(sel_m[:, :R].astype(BF16), normed).astype(BF16)
    xs[...] = chosen.astype(F32).reshape(EXPERTS, SLOT, H).astype(BF16)
    xe_d[0] = normed
    seat = {i: j for j, i in enumerate(NEAR)}
    z_far, z_near = Group(zr.at[pl.ds(3, 5)]), Group(zr.at[pl.ds(1, 2)])
    for i in PACKED[:-1]:
        group = z_far if i in PACKED[:5] else z_near
        group.add(xs.at[(z + i) % Z], zr.at[seat[Z - i]], zpeer[i])
    chunks = [Gather(buf) for buf in (xe_a, xe_b, xe_d)]
    chunks[2].start()
    gate_row = gate_vec[...].astype(F32)
    gate_row = jnp.concatenate([gate_row[r : r + 1] for r in range(H // 128)], axis=1)
    logit = jnp.sum(normed.astype(F32) * gate_row, axis=1, keepdims=True)
    lg_s[...] = logit + jnp.zeros((R, 128), F32)
    c_lg = remote(lg_s, lg_r, partner)
    def new_state(h):
        cols = slice(h * hs, (h + 1) * hs)
        for s in range(R):
            ns[s, h] = decays[h] * st[s, h] + k_t[cols, s : s + 1] * v[s : s + 1, cols]

    new_state(0)

    for name in ("eg", "eu", "ed"):
        local[name].wait()
    for copy in (c_eg, c_eu, c_ed):
        copy.wait_recv()
    for t in range(2):
        for src, dst in ((eg, w1.at[0, t]), (eu, w1.at[1, t]), (ed, w2.at[t])):
            dst[:FE] = src[t]
            dst[FE:] = jnp.zeros((128 - FE, H), BF16)
    weights.start()
    new_state(1)
    comb = [scl_m[(z + i) % Z] for i in NEAR]
    comb.append(jnp.zeros((128 - EXPERTS * SLOT, 128), F32))
    comb = jnp.concatenate(comb, axis=0).T[:R, : EXPERTS * SLOT].astype(BF16)

    xe, pe_o = (xe_a, xe_b, xe_d), (pe_o_a, pe_o_b, pe_o_d)
    pe_s, pe_r = (pe_s_a, pe_s_b, pe_s_d), (pe_r_a, pe_r_b, pe_r_d)
    y32, yb, rb = (y_a, y_b, y_d), (yb_a, yb_b, yb_d), (rb_a, rb_b, rb_d)
    sb, ra = (sb_a, sb_b, sb_d), (ra_a, ra_b, ra_d)
    enter = (w1, w1, w1d)
    leave = (w2, w2, w2d)

    def matches(shape, row_dim, blocks, start):
        row, slot = iota(shape, row_dim) + start, iota(shape, 1 - row_dim)
        found = jnp.zeros(shape, F32)
        for n, j in enumerate(blocks):
            hit = (slot - SLOT * n == row - CAP * j) & (row >= CAP * j) & (row < CAP * (j + 1))
            found = found + jnp.where(hit, 1.0, 0.0)
        return found.astype(BF16)

    def pack(c, blocks, start):
        parts = []
        for j in blocks:
            i = PACKED[j]
            parts.append((zr[seat[i]] if i else xs[z]).astype(F32))
        if len(parts) % 2:
            parts.append(jnp.zeros((SLOT, H), F32))
        rows = jnp.concatenate(parts, axis=0).astype(BF16)
        take = matches((CHUNKS[c], SLOT * len(parts)), 0, blocks, start)
        xe[c][0] = dot(take, rows).astype(BF16)
        chunks[c].start()

    z_far.wait_recv()
    pack(0, (0, 1, 2, 3, 4), 0)
    z_near.wait_recv()
    pack(1, (4, 5, 6, 7), CHUNKS[0])
    chunks[2].go()
    weights.start()
    chunks[0].go()
    chunks[1].go()
    weights.start()

    c_pe, c_rb, c_ra = {}, {}, {}

    def before_act(c):
        n = CHUNKS[c]
        chunks[c].across.wait_recv()
        pre = dot_t(xe[c][...].reshape(PLANE * n, H), enter[c][...].reshape(512, H))
        pe_o[c][...] = pre
        for b in range(SIDE):
            for a in range(SIDE):
                f = SIDE * b + a
                pe_s[c][SIDE * a + b] = pre[f * n : (f + 1) * n].astype(BF16)
        c_pe[c] = remote(pe_s[c], pe_r[c], partner)

    def act(c):
        n = CHUNKS[c]
        c_pe[c].wait_recv()
        pre = pe_o[c][...] + pe_r[c][...].astype(F32).reshape(PLANE * n, 512)
        hidden = (silu(pre[:, :256]) * pre[:, 256:]).astype(BF16)
        down = leave[c][...].reshape(256, H)
        gone = dot(hidden[SIDE * n :], down)
        yb[c][...] = gone.reshape(3 * SIDE, n, H).astype(BF16)
        c_rb[c] = Group(rb[c])
        for d, b in BACK:
            c_rb[c].add(yb[c].at[pl.ds(SIDE * (b - 1), SIDE)], rb[c].at[b - 1], second[d])
        y32[c][...] = dot(hidden[: SIDE * n], down).reshape(SIDE, n, H)

    def sum_second(c):
        c_rb[c].wait_recv()
        total = y32[c][...]
        for b in range(3):
            total = total + rb[c][b].astype(F32)
        sb[c][...] = total[1:].astype(BF16)
        c_ra[c] = Group(ra[c])
        for d, a in BACK:
            c_ra[c].add(sb[c].at[a - 1], ra[c].at[a - 1], first[d])
        y32[c][0] = total[0]

    c_ret = Group(zret.at[pl.ds(1, Z - 1)])

    def sum_first(c):
        c_ra[c].wait_recv()
        total = y32[c][0]
        for a in range(3):
            total = total + ra[c][a].astype(F32)
        return total

    def give_back(c, blocks):
        tot[sum(CHUNKS[:c]) : sum(CHUNKS[: c + 1])] = sum_first(c)
        done = tot[: sum(CHUNKS[: c + 1])]
        pad = -done.shape[0] % 16
        if pad:
            done = jnp.concatenate([done, jnp.zeros((pad, H), F32)], axis=0)
        put = matches((SLOT * len(blocks), done.shape[0]), 1, blocks, 0)
        rows = dot(put, done.astype(BF16))
        for n, j in enumerate(blocks):
            i = PACKED[j]
            block = rows[n * SLOT : (n + 1) * SLOT].astype(BF16)
            if i == 0:
                zret[0] = block
            else:
                zs[i] = block
                c_ret.add(zs.at[i], zret.at[seat[Z - i]], zpeer[i])

    before_act(0)
    act(0)
    before_act(1)
    weights.start()
    for j in range(Z):
        for t, dst in enumerate((w1d.at[0, j], w1d.at[1, j], w2d.at[j])):
            dst[:FD] = wbuf[j, t]
            dst[FD:] = jnp.zeros((32 - FD, H), BF16)
    before_act(2)
    act(1)
    sum_second(0)
    act(2)
    give_back(0, (0, 1, 2, 3))
    sum_second(1)
    sum_second(2)
    give_back(1, (4, 5, 6, 7))
    dense = sum_first(2)

    c_lg.wait_recv()
    open_ = 1.0 / (1.0 + jnp.exp(-(lg_s[:, :1] + lg_r[:, :1])))
    c_ret.wait_recv()
    back = zret[...].astype(F32).reshape(EXPERTS * SLOT, H).astype(BF16)
    moe = dot(comb, back)
    mixed[...] = (after + moe + open_ * dense).astype(BF16)
    for group in sent:
        group.wait_send()
    assert (len(sent), len(local)) == (GROUPS, LOADS), (len(sent), len(local))


def store(a_in, b_in, a_out, b_out, sems):
    first = pltpu.make_async_copy(b_in, b_out, sems.at[0])
    second = pltpu.make_async_copy(a_in, a_out, sems.at[1])
    first.start()
    second.start()
    first.wait()
    second.wait()


def body(
    tokens,
    state,
    norm_mix,
    w_query,
    w_key,
    w_value,
    w_out,
    norm_ffn,
    gate_vector,
    dense_gate,
    dense_up,
    dense_down,
    exp_gate,
    exp_up,
    exp_down,
    routes,
    route_w,
):
    R, H = tokens.shape
    heads, hs = state.shape[1], state.shape[2]
    HW = heads * hs
    FE = exp_gate.shape[2]
    FD = dense_gate.shape[1]
    Z = EXPERTS
    per_chunk = lambda make: [make(n) for n in CHUNKS]
    vm = pl.BlockSpec(memory_space=pltpu.VMEM)
    hbm = pl.BlockSpec(memory_space=pltpu.HBM)
    V = pltpu.VMEM
    sem = lambda *shape: pltpu.SemaphoreType.DMA(shape)
    operands = (
        tokens,
        norm_mix.reshape(1, -1),
        routes.T,
        route_w.T,
        norm_ffn.reshape(1, -1),
        gate_vector.reshape(-1, 128),
        state,
        w_query,
        w_key,
        w_value,
        w_out,
        dense_gate.T,
        dense_up.T,
        dense_down,
        exp_gate[0].T,
        exp_up[0].T,
        exp_down,
    )
    held = [pltpu.with_memory_space_constraint(x, pltpu.HBM) for x in operands]
    mixed, new_state = pl.pallas_call(
        kernel,
        out_shape=(pltpu.VMEM((R, H), BF16), pltpu.VMEM(state.shape, F32)),
        in_specs=[hbm] * 17,
        out_specs=(vm, vm),
        scratch_shapes=[
            V((R, H), BF16),
            V((1, 2 * H), F32),
            V((routes.shape[1], R), jnp.int32),
            V((routes.shape[1], R), BF16),
            V((1, H), F32),
            V((H // 128, 128), BF16),
            V((R, H), BF16),
            V((2, H, HW), BF16),
            V((2, H, HW), BF16),
            V((2, H, HW), BF16),
            V((2, HW, H), BF16),
            V((2, HW, H), BF16),
            V((2, FE, H), BF16),
            V((2, FE, H), BF16),
            V((2, FE, H), BF16),
            V(state.shape, F32),
            V((R, HW), BF16),
            V((R, HW), BF16),
            V((EXPERTS * SLOT, 128), F32),
            V((EXPERTS, SLOT, 128), F32),
            V((R, 128), F32),
            V((R, 128), F32),
            V((Z, 3, FD, H), BF16),
            V((2, 2, 128, H), BF16),
            V((2, 128, H), BF16),
            V((2, Z, 32, H), BF16),
            V((Z, 32, H), BF16),
            V((EXPERTS, SLOT, H), BF16),
            V((Z, SLOT, H), BF16),
            *per_chunk(lambda n: V((PLANE, n, H), BF16)),
            *per_chunk(lambda n: V((PLANE * n, 512), F32)),
            *per_chunk(lambda n: V((PLANE, n, 512), BF16)),
            *per_chunk(lambda n: V((PLANE, n, 512), BF16)),
            *per_chunk(lambda n: V((SIDE, n, H), F32)),
            *per_chunk(lambda n: V((3 * SIDE, n, H), BF16)),
            *per_chunk(lambda n: V((3, SIDE, n, H), BF16)),
            *per_chunk(lambda n: V((3, n, H), BF16)),
            *per_chunk(lambda n: V((3, n, H), BF16)),
            V((sum(CHUNKS[:2]), H), F32),
            V((Z, SLOT, H), BF16),
            V((Z, SLOT, H), BF16),
            sem(LOADS),
            sem(GROUPS),
            sem(GROUPS),
        ],
        compiler_params=pltpu.CompilerParams(
            collective_id=0, has_side_effects=True, vmem_limit_bytes=50 * 1024 * 1024
        ),
        name="layer",
    )(
        *held
    )
    return pl.pallas_call(
        store,
        out_shape=(
            jax.ShapeDtypeStruct((R, H), BF16),
            jax.ShapeDtypeStruct(state.shape, F32),
        ),
        in_specs=[vm, vm],
        out_specs=(hbm, hbm),
        scratch_shapes=[sem(2)],
        name="store",
    )(
        pltpu.with_memory_space_constraint(mixed, pltpu.VMEM),
        pltpu.with_memory_space_constraint(new_state, pltpu.VMEM),
    )


def solution(mesh):
    return jax.shard_map(
        body,
        mesh=mesh,
        in_specs=(
            P("ep", "tp"),
            P("ep", "tp", None, None),
            P(),
            P(None, "tp"),
            P(None, "tp"),
            P(None, "tp"),
            P("tp", None),
            P("tp"),
            P("tp"),
            P("tp", "ep"),
            P("tp", "ep"),
            P("ep", "tp"),
            P("ep", None, "tp"),
            P("ep", None, "tp"),
            P("ep", "tp", None),
            P("ep", None),
            P("ep", None),
        ),
        out_specs=(P("ep", "tp"), P("ep", "tp", None, None)),
        check_vma=False,
    )
```

time: 63.7 us -> 55.7 us (0.87); the launches traced: 62.8 us -> 55.6 us
  Pallas kernels: 62.1 us -> 54.9 us
    pallas_call x1, Pallas kernels: 60.8 us -> 53.6 us  [body(): pl.pallas_call(kernel, out_shape=(pltpu.VMEM((R, H), BF16), pltpu.VMEM(st...]
where the time goes in v3:
time: 55.7 us; the launch traced here: 55.6 us
  Pallas kernels  54.9 us (99%)
  between operations  0.65 us (1%)
    pallas_call x1, Pallas kernels, body(): pl.pallas_call(kernel, out_shape=(pltpu.VMEM((R, H), BF16), pltpu.VMEM(st...  53.6 us
    pallas_call x1, Pallas kernels, body(): pl.pallas_call(store, out_shape=(jax.ShapeDtypeStruct((R, H), BF16), jax....  1.34 us

profile of v3, /device:TPU:1, one launch (start us, length us, event | category | flops | bytes accessed | tf_op | source)
XLA Modules:
  0.0 55.6 jit_solution(11784535354398243743)
XLA Ops:
  0.6 53.6 %layer.1 = (bf16[16,1024]{1,0:T(8,128)(2,1)S(1)}, f32[16,2,128,128]{3,2,1,0:T(8,128)S(1)}) custom-call(bf16[16,1024]{1,0:T(8,128)(2,1)} %tokens_h.1, f32[1,2048]{1,0:T(1,128)} %bitcast.17, s32[2,16]{1,0:T(2,128)} %bitcast.20, bf16[2,16]{1,0:T(2,128)(2,1)} %bitcast.21, f32[1,1024]{1,0:T(1,128)} %bitcast.18, bf16[8,128]{1,0:T(8,128)(2,1)} %bitcast.19, ...), custom_call_target="tpu_custom_call" | custom-call | tf_op jit(solution)/shard_map/layer/pallas_call | solution.py:586
  54.2 1.3 %store.1 = (bf16[16,1024]{1,0:T(8,128)(2,1)}, f32[16,2,128,128]{3,2,1,0:T(8,128)}) custom-call(bf16[16,1024]{1,0:T(8,128)(2,1)S(1)} %get-tuple-element.4.a_in, f32[16,2,128,128]{3,2,1,0:T(8,128)S(1)} %get-tuple-element.5.b_in), custom_call_target="tpu_custom_call" | custom-call | tf_op jit(solution)/shard_map/store/pallas_call | solution.py:644

commit v4 on v3

--- a/solution.py
+++ b/solution.py
@@ -13,9 +13,16 @@
 SIDE = 4
 PLANE = SIDE * SIDE
 NEAR = (0, 1, 7, 2, 6, 3, 5, 4)
-PACKED = (4, 3, 5, 2, 6, 1, 7, 0)
-CHUNKS = (24, 16, 16)
-GROUPS = 32
+TRIPS = (
+    ((1, 0, CAP), (2, 0, CAP), (6, 0, CAP), (7, 0, 1)),
+    ((3, 0, CAP), (4, 0, CAP), (5, 0, CAP), (7, 1, 1)),
+    ((7, 2, CAP - 2), (0, 0, CAP)),
+)
+CHUNKS = (16, 16, 8, 16)
+DENSE = len(CHUNKS) - 1
+RELAY_IN = ()
+RELAY_OUT = ()
+GROUPS = 38 + len(RELAY_IN) + len(RELAY_OUT)
 LOADS = 21
 epsilon = 1e-06
 MESH = pl.DeviceIdType.MESH
@@ -90,30 +97,39 @@
     zr,
     xe_a,
     xe_b,
+    xe_c,
     xe_d,
     pe_o_a,
     pe_o_b,
+    pe_o_c,
     pe_o_d,
     pe_s_a,
     pe_s_b,
+    pe_s_c,
     pe_s_d,
     pe_r_a,
     pe_r_b,
+    pe_r_c,
     pe_r_d,
     y_a,
     y_b,
+    y_c,
     y_d,
     yb_a,
     yb_b,
+    yb_c,
     yb_d,
     rb_a,
     rb_b,
+    rb_c,
     rb_d,
     sb_a,
     sb_b,
+    sb_c,
     sb_d,
     ra_a,
     ra_b,
+    ra_c,
     ra_d,
     tot,
     zs,
@@ -191,28 +207,34 @@
     BACK = ((2, 3), (-1, 1), (1, 2))
 
     class Gather:
-        def __init__(self, buf):
-            self.at = buf.at
+        def __init__(self, buf, relayed):
+            self.at, self.relayed = buf.at, relayed
 
         def spread(self, *todo):
-            for d, b in HOPS:
+            for d, b in HOPS[:2] if self.relayed else HOPS:
                 for a in todo:
                     self.across.add(self.at[a], self.at[SIDE * b + a], second[d])
 
         def start(self):
             at = self.at
             self.near, self.far = Group(at[pl.ds(1, 2)]), Group(at[3])
-            self.across = Group(at[pl.ds(SIDE, 3 * SIDE)])
+            self.across = Group(at[pl.ds(SIDE, (2 if self.relayed else 3) * SIDE)])
             self.near.add(at[0], at[1], first[1])
             self.near.add(at[0], at[2], first[-1])
             self.far.add(at[0], at[3], first[2])
-            self.spread(0)
 
         def go(self):
             self.near.wait_recv()
             self.spread(1, 2)
             self.far.wait_recv()
             self.spread(3)
+
+        def relay(self):
+            at = self.at
+            self.across.wait_recv()
+            self.across = Group(at[pl.ds(3 * SIDE, SIDE)])
+            for a, b, d in ((0, 1, 1), (1, 1, 1), (2, 2, -1), (3, 2, -1)):
+                self.across.add(at[SIDE * b + a], at[3 * SIDE + a], second[d])
 
     class Ring:
         def __init__(self, buf):
@@ -363,12 +385,14 @@
     xs[...] = chosen.astype(F32).reshape(EXPERTS, SLOT, H).astype(BF16)
     xe_d[0] = normed
     seat = {i: j for j, i in enumerate(NEAR)}
-    z_far, z_near = Group(zr.at[pl.ds(3, 5)]), Group(zr.at[pl.ds(1, 2)])
-    for i in PACKED[:-1]:
-        group = z_far if i in PACKED[:5] else z_near
+    z_near, z_far = Group(zr.at[pl.ds(1, 4)]), Group(zr.at[pl.ds(5, 3)])
+    for i in (2, 6, 1, 7, 4, 3, 5):
+        group = z_near if i in NEAR[:5] else z_far
         group.add(xs.at[(z + i) % Z], zr.at[seat[Z - i]], zpeer[i])
-    chunks = [Gather(buf) for buf in (xe_a, xe_b, xe_d)]
-    chunks[2].start()
+    xe = (xe_a, xe_b, xe_c, xe_d)
+    chunks = [Gather(buf, c in RELAY_IN) for c, buf in enumerate(xe)]
+    chunks[DENSE].start()
+    chunks[DENSE].spread(0)
     gate_row = gate_vec[...].astype(F32)
     gate_row = jnp.concatenate([gate_row[r : r + 1] for r in range(H // 128)], axis=1)
     logit = jnp.sum(normed.astype(F32) * gate_row, axis=1, keepdims=True)
@@ -389,50 +413,57 @@
         for src, dst in ((eg, w1.at[0, t]), (eu, w1.at[1, t]), (ed, w2.at[t])):
             dst[:FE] = src[t]
             dst[FE:] = jnp.zeros((128 - FE, H), BF16)
-    weights.start()
     new_state(1)
     comb = [scl_m[(z + i) % Z] for i in NEAR]
     comb.append(jnp.zeros((128 - EXPERTS * SLOT, 128), F32))
     comb = jnp.concatenate(comb, axis=0).T[:R, : EXPERTS * SLOT].astype(BF16)
 
-    xe, pe_o = (xe_a, xe_b, xe_d), (pe_o_a, pe_o_b, pe_o_d)
-    pe_s, pe_r = (pe_s_a, pe_s_b, pe_s_d), (pe_r_a, pe_r_b, pe_r_d)
-    y32, yb, rb = (y_a, y_b, y_d), (yb_a, yb_b, yb_d), (rb_a, rb_b, rb_d)
-    sb, ra = (sb_a, sb_b, sb_d), (ra_a, ra_b, ra_d)
-    enter = (w1, w1, w1d)
-    leave = (w2, w2, w2d)
-
-    def matches(shape, row_dim, blocks, start):
-        row, slot = iota(shape, row_dim) + start, iota(shape, 1 - row_dim)
-        found = jnp.zeros(shape, F32)
-        for n, j in enumerate(blocks):
-            hit = (slot - SLOT * n == row - CAP * j) & (row >= CAP * j) & (row < CAP * (j + 1))
-            found = found + jnp.where(hit, 1.0, 0.0)
+    pe_o = (pe_o_a, pe_o_b, pe_o_c, pe_o_d)
+    pe_s = (pe_s_a, pe_s_b, pe_s_c, pe_s_d)
+    pe_r = (pe_r_a, pe_r_b, pe_r_c, pe_r_d)
+    y32, yb = (y_a, y_b, y_c, y_d), (yb_a, yb_b, yb_c, yb_d)
+    rb, sb = (rb_a, rb_b, rb_c, rb_d), (sb_a, sb_b, sb_c, sb_d)
+    ra = (ra_a, ra_b, ra_c, ra_d)
+    enter = (w1, w1, w1, w1d)
+    leave = (w2, w2, w2, w2d)
+
+    def matches(shape, row_dim, order, trips):
+        row, slot = iota(shape, row_dim), iota(shape, 1 - row_dim)
+        found, first_row = jnp.zeros(shape, F32), 0
+        for i, first_slot, count in trips:
+            if i in order:
+                shift = SLOT * order.index(i) + first_slot - first_row
+                hit = (slot - row == shift) & (row >= first_row) & (row < first_row + count)
+                found = found + jnp.where(hit, 1.0, 0.0)
+            first_row += count
         return found.astype(BF16)
 
-    def pack(c, blocks, start):
-        parts = []
-        for j in blocks:
-            i = PACKED[j]
-            parts.append((zr[seat[i]] if i else xs[z]).astype(F32))
+    def pack(c):
+        order = [i for i, _, _ in TRIPS[c]]
+        parts = [(zr[seat[i]] if i else xs[z]).astype(F32) for i in order]
         if len(parts) % 2:
             parts.append(jnp.zeros((SLOT, H), F32))
         rows = jnp.concatenate(parts, axis=0).astype(BF16)
-        take = matches((CHUNKS[c], SLOT * len(parts)), 0, blocks, start)
+        take = matches((CHUNKS[c], SLOT * len(parts)), 0, order, TRIPS[c])
         xe[c][0] = dot(take, rows).astype(BF16)
         chunks[c].start()
 
+    z_near.wait_recv()
+    pack(0)
+    pack(2)
+    chunks[0].spread(0)
+    chunks[2].spread(0)
+    weights.start()
+    chunks[DENSE].go()
     z_far.wait_recv()
-    pack(0, (0, 1, 2, 3, 4), 0)
-    z_near.wait_recv()
-    pack(1, (4, 5, 6, 7), CHUNKS[0])
+    pack(1)
+    chunks[1].spread(0)
+    chunks[0].go()
     chunks[2].go()
     weights.start()
-    chunks[0].go()
     chunks[1].go()
-    weights.start()
-
-    c_pe, c_rb, c_ra = {}, {}, {}
+
+    c_pe, c_rx, c_rb, c_ra = {}, {}, {}, {}
 
     def before_act(c):
         n = CHUNKS[c]
@@ -453,15 +484,34 @@
         down = leave[c][...].reshape(256, H)
         gone = dot(hidden[SIDE * n :], down)
         yb[c][...] = gone.reshape(3 * SIDE, n, H).astype(BF16)
-        c_rb[c] = Group(rb[c])
-        for d, b in BACK:
-            c_rb[c].add(yb[c].at[pl.ds(SIDE * (b - 1), SIDE)], rb[c].at[b - 1], second[d])
+        out, at = yb[c].at, rb[c].at
+        if c in RELAY_OUT:
+            low, high = pl.ds(0, 2), pl.ds(2, 2)
+            c_rx[c] = Group(at[2])
+            c_rx[c].add(out[pl.ds(2 * SIDE, 2)], at[2, low], second[1])
+            c_rx[c].add(out[pl.ds(2 * SIDE + 2, 2)], at[2, high], second[-1])
+            c_rb[c] = Group(at[pl.ds(0, 2)])
+            c_rb[c].add(out[pl.ds(SIDE + 2, 2)], at[0, high], second[1])
+            c_rb[c].add(out[low], at[1, low], second[-1])
+        else:
+            c_rb[c] = Group(rb[c])
+            for d, b in BACK:
+                c_rb[c].add(out[pl.ds(SIDE * (b - 1), SIDE)], at[b - 1], second[d])
         y32[c][...] = dot(hidden[: SIDE * n], down).reshape(SIDE, n, H)
+
+    def sum_relay(c):
+        c_rx[c].wait_recv()
+        n, out, at = CHUNKS[c], yb[c], rb[c].at
+        for half, slot, d in ((0, SIDE, 1), (1, 2, -1)):
+            here, part = pl.ds(slot, 2), pl.ds(2 * half, 2)
+            more = out[slot : slot + 2].astype(F32) + rb[c][2, 2 * half : 2 * half + 2].astype(F32)
+            out[slot : slot + 2] = more.astype(BF16)
+            c_rb[c].add(out.at[here], at[half, part], second[d])
 
     def sum_second(c):
         c_rb[c].wait_recv()
         total = y32[c][...]
-        for b in range(3):
+        for b in range(2 if c in RELAY_OUT else 3):
             total = total + rb[c][b].astype(F32)
         sb[c][...] = total[1:].astype(BF16)
         c_ra[c] = Group(ra[c])
@@ -478,16 +528,15 @@
             total = total + ra[c][a].astype(F32)
         return total
 
-    def give_back(c, blocks):
+    def give_back(c, *order):
         tot[sum(CHUNKS[:c]) : sum(CHUNKS[: c + 1])] = sum_first(c)
         done = tot[: sum(CHUNKS[: c + 1])]
         pad = -done.shape[0] % 16
         if pad:
             done = jnp.concatenate([done, jnp.zeros((pad, H), F32)], axis=0)
-        put = matches((SLOT * len(blocks), done.shape[0]), 1, blocks, 0)
+        put = matches((SLOT * len(order), done.shape[0]), 1, order, sum(TRIPS[: c + 1], ()))
         rows = dot(put, done.astype(BF16))
-        for n, j in enumerate(blocks):
-            i = PACKED[j]
+        for n, i in enumerate(order):
             block = rows[n * SLOT : (n + 1) * SLOT].astype(BF16)
             if i == 0:
                 zret[0] = block
@@ -496,22 +545,27 @@
                 c_ret.add(zs.at[i], zret.at[seat[Z - i]], zpeer[i])
 
     before_act(0)
+    weights.start()
     act(0)
     before_act(1)
+    before_act(2)
+    act(1)
     weights.start()
     for j in range(Z):
         for t, dst in enumerate((w1d.at[0, j], w1d.at[1, j], w2d.at[j])):
             dst[:FD] = wbuf[j, t]
             dst[FD:] = jnp.zeros((32 - FD, H), BF16)
-    before_act(2)
-    act(1)
+    before_act(DENSE)
+    act(2)
     sum_second(0)
-    act(2)
-    give_back(0, (0, 1, 2, 3))
+    act(DENSE)
     sum_second(1)
+    give_back(0, 1, 2, 6)
     sum_second(2)
-    give_back(1, (4, 5, 6, 7))
-    dense = sum_first(2)
+    give_back(1, 3, 4, 5)
+    sum_second(DENSE)
+    give_back(2, 7, 0)
+    dense = sum_first(DENSE)
 
     c_lg.wait_recv()
     open_ = 1.0 / (1.0 + jnp.exp(-(lg_s[:, :1] + lg_r[:, :1])))
@@ -627,7 +681,7 @@
             *per_chunk(lambda n: V((3, SIDE, n, H), BF16)),
             *per_chunk(lambda n: V((3, n, H), BF16)),
             *per_chunk(lambda n: V((3, n, H), BF16)),
-            V((sum(CHUNKS[:2]), H), F32),
+            V((sum(CHUNKS[:DENSE]), H), F32),
             V((Z, SLOT, H), BF16),
             V((Z, SLOT, H), BF16),
             sem(LOADS),

time: 55.7 us -> 52.1 us (0.935)
  Pallas kernels: 54.9 us -> 51.4 us
    pallas_call x1, Pallas kernels: 53.6 us -> 50.1 us  [body(): pl.pallas_call(kernel, out_shape=(pltpu.VMEM((R, H), BF16), pltpu.VMEM(st...]
where the time goes in v4:
time: 52.1 us
  Pallas kernels  51.4 us (99%)
  between operations  0.65 us (1%)
    pallas_call x1, Pallas kernels, body(): pl.pallas_call(kernel, out_shape=(pltpu.VMEM((R, H), BF16), pltpu.VMEM(st...  50.1 us
    pallas_call x1, Pallas kernels, body(): pl.pallas_call(store, out_shape=(jax.ShapeDtypeStruct((R, H), BF16), jax....  1.34 us

profile of v4, /device:TPU:1, one launch (start us, length us, event | category | flops | bytes accessed | tf_op | source)
XLA Modules:
  0.0 52.1 jit_solution(2343960100771845350)
XLA Ops:
  0.6 50.1 %layer.1 = (bf16[16,1024]{1,0:T(8,128)(2,1)S(1)}, f32[16,2,128,128]{3,2,1,0:T(8,128)S(1)}) custom-call(bf16[16,1024]{1,0:T(8,128)(2,1)} %tokens_h.1, f32[1,2048]{1,0:T(1,128)} %bitcast.17, s32[2,16]{1,0:T(2,128)} %bitcast.20, bf16[2,16]{1,0:T(2,128)(2,1)} %bitcast.21, f32[1,1024]{1,0:T(1,128)} %bitcast.18, bf16[8,128]{1,0:T(8,128)(2,1)} %bitcast.19, ...), custom_call_target="tpu_custom_call" | custom-call | tf_op jit(solution)/shard_map/layer/pallas_call | solution.py:640
  50.7 1.3 %store.1 = (bf16[16,1024]{1,0:T(8,128)(2,1)}, f32[16,2,128,128]{3,2,1,0:T(8,128)}) custom-call(bf16[16,1024]{1,0:T(8,128)(2,1)S(1)} %get-tuple-element.4.a_in, f32[16,2,128,128]{3,2,1,0:T(8,128)S(1)} %get-tuple-element.5.b_in), custom_call_target="tpu_custom_call" | custom-call | tf_op jit(solution)/shard_map/store/pallas_call | solution.py:698

commit v5 on v4

--- a/solution.py
+++ b/solution.py
@@ -20,10 +20,9 @@
 )
 CHUNKS = (16, 16, 8, 16)
 DENSE = len(CHUNKS) - 1
-RELAY_IN = ()
-RELAY_OUT = ()
-GROUPS = 38 + len(RELAY_IN) + len(RELAY_OUT)
-LOADS = 21
+GROUPS = 36
+SENDS = 24
+LOADS = 17
 epsilon = 1e-06
 MESH = pl.DeviceIdType.MESH
 F32 = jnp.float32
@@ -78,9 +77,7 @@
     wv,
     wo_o,
     wo_p,
-    eg,
-    eu,
-    ed,
+    we,
     st,
     ho_o,
     ho_p,
@@ -137,12 +134,13 @@
     lsem,
     ssem,
     rsem,
+    gsem,
 ):
     R, H = tokens.shape
     D = 2 * H
     heads, hs = state.shape[1], state.shape[2]
     HW = heads * hs
-    FE = eg.shape[1]
+    FE = we.shape[2]
     FD = wbuf.shape[2]
     Z = EXPERTS
     me = lax.axis_index("ep")
@@ -164,19 +162,20 @@
     own = pl.ds(pl.multiple_of(tp * H, H), H)
     oth = pl.ds(pl.multiple_of(other * H, H), H)
 
-    sent = []
+    sent, groups = [], []
 
     class Group:
-        def __init__(self, whole):
-            self.k, self.whole = len(sent), whole
-            sent.append(self)
+        def __init__(self, whole, out=None):
+            self.whole = whole
+            self.k = groups.append(self) or len(groups) - 1
+            self.out = sent.append(self) or len(sent) - 1 if out is None else out.out
 
         def copy(self, src, dst, dev):
             self.dev = dev
             return pltpu.make_async_remote_copy(
                 src_ref=src,
                 dst_ref=dst,
-                send_sem=ssem.at[self.k],
+                send_sem=ssem.at[self.out],
                 recv_sem=rsem.at[self.k],
                 device_id=dev,
                 device_id_type=MESH,
@@ -191,6 +190,21 @@
         def wait_send(self):
             self.copy(self.whole, self.whole, self.dev).wait_send()
 
+    class Sends:
+        def __init__(self, whole, dev):
+            self.whole, self.dev = whole, dev
+            self.out = sent.append(self) or len(sent) - 1
+
+        def wait_send(self):
+            pltpu.make_async_remote_copy(
+                src_ref=self.whole,
+                dst_ref=self.whole,
+                send_sem=ssem.at[self.out],
+                recv_sem=rsem.at[0],
+                device_id=self.dev,
+                device_id_type=MESH,
+            ).wait_send()
+
     def remote(src, dst, dev):
         group = Group(dst)
         group.add(src, dst, dev)
@@ -203,25 +217,26 @@
         copy.start()
         local[name] = copy
 
-    HOPS = ((1, 1), (-1, 2), (2, 3))
+    HOPS = ((2, 3), (1, 1), (-1, 2))
     BACK = ((2, 3), (-1, 1), (1, 2))
 
     class Gather:
-        def __init__(self, buf, relayed):
-            self.at, self.relayed = buf.at, relayed
+        def __init__(self, buf):
+            self.at = buf.at
 
         def spread(self, *todo):
-            for d, b in HOPS[:2] if self.relayed else HOPS:
+            for d, b in HOPS:
                 for a in todo:
                     self.across.add(self.at[a], self.at[SIDE * b + a], second[d])
 
         def start(self):
             at = self.at
-            self.near, self.far = Group(at[pl.ds(1, 2)]), Group(at[3])
-            self.across = Group(at[pl.ds(SIDE, (2 if self.relayed else 3) * SIDE)])
+            out = Sends(at[pl.ds(1, PLANE - 1)], partner)
+            self.near, self.far = Group(at[pl.ds(1, 2)], out), Group(at[3], out)
+            self.across = Group(at[pl.ds(SIDE, 3 * SIDE)], out)
+            self.far.add(at[0], at[3], first[2])
             self.near.add(at[0], at[1], first[1])
             self.near.add(at[0], at[2], first[-1])
-            self.far.add(at[0], at[3], first[2])
 
         def go(self):
             self.near.wait_recv()
@@ -229,16 +244,10 @@
             self.far.wait_recv()
             self.spread(3)
 
-        def relay(self):
-            at = self.at
-            self.across.wait_recv()
-            self.across = Group(at[pl.ds(3 * SIDE, SIDE)])
-            for a, b, d in ((0, 1, 1), (1, 1, 1), (2, 2, -1), (3, 2, -1)):
-                self.across.add(at[SIDE * b + a], at[3 * SIDE + a], second[d])
-
     class Ring:
         def __init__(self, buf):
             self.at, self.step = buf.at, 0
+            self.out = Sends(buf.at[pl.ds(1, Z - 1)], partner)
 
         def start(self):
             at, t = self.at, self.step
@@ -246,11 +255,11 @@
                 self.group.wait_recv()
             up, down = max(0, 2 * t), max(0, 2 * t - 1)
             if t < 3:
-                self.group = Group(at[pl.ds(2 * t + 1, 2)])
+                self.group = Group(at[pl.ds(2 * t + 1, 2)], self.out)
                 self.group.add(at[up], at[2 * t + 2], zpeer[1])
                 self.group.add(at[down], at[2 * t + 1], zpeer[-1])
             elif t == 3:
-                self.group = Group(at[7])
+                self.group = Group(at[7], self.out)
                 self.group.add(at[up, pl.ds(0, 2)], at[7, pl.ds(0, 2)], zpeer[1])
                 self.group.add(at[down, pl.ds(2, 1)], at[7, pl.ds(2, 1)], zpeer[-1])
             self.step = t + 1
@@ -264,26 +273,34 @@
         (gate_vec_h, gate_vec),
     )
     barrier = pltpu.get_barrier_semaphore()
-    greeted = [partner, *first.values(), *second.values()] + zpeer[1:]
+    greeted = [partner, first[1], first[-1], second[1], second[-1], zpeer[1], zpeer[-1]]
+    load("s0", tokens_h, tokens)
     for dev in greeted:
         pl.semaphore_signal(barrier, inc=1, device_id=dev, device_id_type=MESH)
 
     for t, (src, dst) in enumerate(small):
-        load(f"s{t}", src, dst)
+        if t:
+            load(f"s{t}", src, dst)
     for t, src in enumerate((dense_gate, dense_up, dense_down)):
         load(f"d{t}", src, wbuf.at[0, t])
     for t, (src, dst) in enumerate(((w_query, wq), (w_key, wk), (w_value, wv))):
-        load(f"p{t}o", src.at[own, :], dst.at[0])
-        load(f"p{t}p", src.at[oth, :], dst.at[1])
+        load(f"p{t}", src, dst)
     load("st", state, st)
-    load("wo0", w_out.at[:, own], wo_o.at[0])
-    load("wo1", w_out.at[:, oth], wo_o.at[1])
-    load("eg", exp_gate.at[:, own], eg.at[tp])
-    load("eu", exp_up.at[:, own], eu.at[tp])
-    load("ed", exp_down.at[0, :, own], ed.at[tp])
+    load("wo", w_out, wo_o)
+    load("eg", exp_gate.at[:, own], we.at[tp, 0])
+    load("eu", exp_up.at[:, own], we.at[tp, 1])
+    load("ed", exp_down.at[0, :, own], we.at[tp, 2])
 
     local["s0"].wait()
     pl.semaphore_wait(barrier, len(greeted))
+
+    def tell(k, *devs):
+        for dev in devs:
+            pl.semaphore_signal(gsem.at[k], inc=1, device_id=dev, device_id_type=MESH)
+
+    tell(0, first[-1])
+    tell(1, second[-1])
+    tell(2, zpeer[1], zpeer[-1])
 
     c_tok = remote(tokens, tok_p, partner)
     weights = Ring(wbuf)
@@ -293,9 +310,9 @@
     c_wo = Group(wo_p)
     c_wo.add(w_out.at[:, oth], wo_p.at[0], partner)
     c_wo.add(w_out.at[:, own], wo_p.at[1], partner)
-    c_eg = remote(exp_gate.at[:, oth], eg.at[tp], partner)
-    c_eu = remote(exp_up.at[:, oth], eu.at[tp], partner)
-    c_ed = remote(exp_down.at[0, :, oth], ed.at[tp], partner)
+    c_we = Group(we.at[tp])
+    for t, src in enumerate((exp_gate.at[:, oth], exp_up.at[:, oth], exp_down.at[0, :, oth])):
+        c_we.add(src, we.at[tp, t], partner)
 
     for t in (2, 3):
         local[f"s{t}"].wait()
@@ -334,19 +351,23 @@
     gain_p = norm_mix[:, oth]
     nx_o = (tok_f * scale * gain_o).astype(BF16)
     nx_p = (tok_pf * scale * gain_p).astype(BF16)
-    proj = []
-    for t, w in enumerate((wq, wk, wv)):
-        local[f"p{t}o"].wait()
-        part = dot(nx_o, w[0])
-        local[f"p{t}p"].wait()
-        proj.append((part + dot(nx_p, w[1])).astype(BF16).astype(F32))
-    q, k, v = proj
-    k = k * hs ** (-0.5)
+
+    def project(w):
+        return (dot(nx_o, w[own, :]) + dot(nx_p, w[oth, :])).astype(BF16).astype(F32)
+
+    local["p0"].wait()
+    q = project(wq)
     pad = jnp.zeros((128 - R, HW), F32)
     q_t = jnp.concatenate([q, pad], axis=0).T
+    pl.semaphore_wait(gsem.at[2], 2)
+    tell(3, zpeer[2], zpeer[-2])
+    for t in (1, 2):
+        local[f"p{t}"].wait()
+    local["st"].wait()
+    k = project(wk) * hs ** (-0.5)
+    v = project(wv)
     k_t = jnp.concatenate([k, pad], axis=0).T
     head_id = tp * heads
-    local["st"].wait()
     decays = []
     for h in range(heads):
         cols = slice(h * hs, (h + 1) * hs)
@@ -365,10 +386,9 @@
         ho_o[:, cols] = (dev * lax.rsqrt(spread + epsilon)).astype(BF16)
     c_ho = remote(ho_o, ho_p, partner)
     ho = ho_o[...]
-    local["wo0"].wait()
-    local["wo1"].wait()
-    a_o = dot(ho, wo_o[0]).astype(BF16).astype(F32)
-    a_p = dot(ho, wo_o[1]).astype(BF16).astype(F32)
+    local["wo"].wait()
+    a_o = dot(ho, wo_o[:, own]).astype(BF16).astype(F32)
+    a_p = dot(ho, wo_o[:, oth]).astype(BF16).astype(F32)
     c_wo.wait_recv()
     c_ho.wait_recv()
     hp = ho_p[...]
@@ -381,16 +401,20 @@
     )
     normed = (after * lax.rsqrt(squares / D + epsilon) * norm_ffn[...]).astype(BF16)
 
+    pl.semaphore_wait(gsem.at[0], 1)
+    pl.semaphore_wait(gsem.at[1], 1)
+    pl.semaphore_wait(gsem.at[3], 2)
     chosen = dot(sel_m[:, :R].astype(BF16), normed).astype(BF16)
     xs[...] = chosen.astype(F32).reshape(EXPERTS, SLOT, H).astype(BF16)
     xe_d[0] = normed
     seat = {i: j for j, i in enumerate(NEAR)}
-    z_near, z_far = Group(zr.at[pl.ds(1, 4)]), Group(zr.at[pl.ds(5, 3)])
+    z_out = Sends(zr.at[pl.ds(1, Z - 1)], partner)
+    z_near, z_far = Group(zr.at[pl.ds(1, 4)], z_out), Group(zr.at[pl.ds(5, 3)], z_out)
     for i in (2, 6, 1, 7, 4, 3, 5):
         group = z_near if i in NEAR[:5] else z_far
         group.add(xs.at[(z + i) % Z], zr.at[seat[Z - i]], zpeer[i])
     xe = (xe_a, xe_b, xe_c, xe_d)
-    chunks = [Gather(buf, c in RELAY_IN) for c, buf in enumerate(xe)]
+    chunks = [Gather(buf) for buf in xe]
     chunks[DENSE].start()
     chunks[DENSE].spread(0)
     gate_row = gate_vec[...].astype(F32)
@@ -407,11 +431,10 @@
 
     for name in ("eg", "eu", "ed"):
         local[name].wait()
-    for copy in (c_eg, c_eu, c_ed):
-        copy.wait_recv()
+    c_we.wait_recv()
     for t in range(2):
-        for src, dst in ((eg, w1.at[0, t]), (eu, w1.at[1, t]), (ed, w2.at[t])):
-            dst[:FE] = src[t]
+        for n, dst in enumerate((w1.at[0, t], w1.at[1, t], w2.at[t])):
+            dst[:FE] = we[t, n]
             dst[FE:] = jnp.zeros((128 - FE, H), BF16)
     new_state(1)
     comb = [scl_m[(z + i) % Z] for i in NEAR]
@@ -463,7 +486,7 @@
     weights.start()
     chunks[1].go()
 
-    c_pe, c_rx, c_rb, c_ra = {}, {}, {}, {}
+    c_pe, c_rb, c_ra = {}, {}, {}
 
     def before_act(c):
         n = CHUNKS[c]
@@ -485,33 +508,15 @@
         gone = dot(hidden[SIDE * n :], down)
         yb[c][...] = gone.reshape(3 * SIDE, n, H).astype(BF16)
         out, at = yb[c].at, rb[c].at
-        if c in RELAY_OUT:
-            low, high = pl.ds(0, 2), pl.ds(2, 2)
-            c_rx[c] = Group(at[2])
-            c_rx[c].add(out[pl.ds(2 * SIDE, 2)], at[2, low], second[1])
-            c_rx[c].add(out[pl.ds(2 * SIDE + 2, 2)], at[2, high], second[-1])
-            c_rb[c] = Group(at[pl.ds(0, 2)])
-            c_rb[c].add(out[pl.ds(SIDE + 2, 2)], at[0, high], second[1])
-            c_rb[c].add(out[low], at[1, low], second[-1])
-        else:
-            c_rb[c] = Group(rb[c])
-            for d, b in BACK:
-                c_rb[c].add(out[pl.ds(SIDE * (b - 1), SIDE)], at[b - 1], second[d])
+        c_rb[c] = Group(rb[c])
+        for d, b in BACK:
+            c_rb[c].add(out[pl.ds(SIDE * (b - 1), SIDE)], at[b - 1], second[d])
         y32[c][...] = dot(hidden[: SIDE * n], down).reshape(SIDE, n, H)
-
-    def sum_relay(c):
-        c_rx[c].wait_recv()
-        n, out, at = CHUNKS[c], yb[c], rb[c].at
-        for half, slot, d in ((0, SIDE, 1), (1, 2, -1)):
-            here, part = pl.ds(slot, 2), pl.ds(2 * half, 2)
-            more = out[slot : slot + 2].astype(F32) + rb[c][2, 2 * half : 2 * half + 2].astype(F32)
-            out[slot : slot + 2] = more.astype(BF16)
-            c_rb[c].add(out.at[here], at[half, part], second[d])
 
     def sum_second(c):
         c_rb[c].wait_recv()
         total = y32[c][...]
-        for b in range(2 if c in RELAY_OUT else 3):
+        for b in range(3):
             total = total + rb[c][b].astype(F32)
         sb[c][...] = total[1:].astype(BF16)
         c_ra[c] = Group(ra[c])
@@ -575,7 +580,7 @@
     mixed[...] = (after + moe + open_ * dense).astype(BF16)
     for group in sent:
         group.wait_send()
-    assert (len(sent), len(local)) == (GROUPS, LOADS), (len(sent), len(local))
+    assert (len(groups), len(sent), len(local)) == (GROUPS, SENDS, LOADS), (len(groups), len(sent))
 
 
 def store(a_in, b_in, a_out, b_out, sems):
@@ -650,14 +655,12 @@
             V((1, H), F32),
             V((H // 128, 128), BF16),
             V((R, H), BF16),
-            V((2, H, HW), BF16),
-            V((2, H, HW), BF16),
-            V((2, H, HW), BF16),
+            V((2 * H, HW), BF16),
+            V((2 * H, HW), BF16),
+            V((2 * H, HW), BF16),
+            V((HW, 2 * H), BF16),
             V((2, HW, H), BF16),
-            V((2, HW, H), BF16),
-            V((2, FE, H), BF16),
-            V((2, FE, H), BF16),
-            V((2, FE, H), BF16),
+            V((2, 3, FE, H), BF16),
             V(state.shape, F32),
             V((R, HW), BF16),
             V((R, HW), BF16),
@@ -685,8 +688,9 @@
             V((Z, SLOT, H), BF16),
             V((Z, SLOT, H), BF16),
             sem(LOADS),
+            sem(SENDS),
             sem(GROUPS),
-            sem(GROUPS),
+            pltpu.SemaphoreType.REGULAR((4,)),
         ],
         compiler_params=pltpu.CompilerParams(
             collective_id=0, has_side_effects=True, vmem_limit_bytes=50 * 1024 * 1024

time: 52.1 us -> 51 us (0.979)
  Pallas kernels: 51.4 us -> 50.3 us
    pallas_call x1, Pallas kernels: 50.1 us -> 48.9 us  [body(): pl.pallas_call(kernel, out_shape=(pltpu.VMEM((R, H), BF16), pltpu.VMEM(st...]
where the time goes in v5:
time: 51 us; the launch traced here: 50.9 us
  Pallas kernels  50.3 us (99%)
  between operations  0.65 us (1%)
    pallas_call x1, Pallas kernels, body(): pl.pallas_call(kernel, out_shape=(pltpu.VMEM((R, H), BF16), pltpu.VMEM(st...  48.9 us
    pallas_call x1, Pallas kernels, body(): pl.pallas_call(store, out_shape=(jax.ShapeDtypeStruct((R, H), BF16), jax....  1.34 us

profile of v5, /device:TPU:1, one launch (start us, length us, event | category | flops | bytes accessed | tf_op | source)
XLA Modules:
  0.0 50.9 jit_solution(6731864451070810832)
XLA Ops:
  0.6 48.9 %layer.1 = (bf16[16,1024]{1,0:T(8,128)(2,1)S(1)}, f32[16,2,128,128]{3,2,1,0:T(8,128)S(1)}) custom-call(bf16[16,1024]{1,0:T(8,128)(2,1)} %tokens_h.1, f32[1,2048]{1,0:T(1,128)} %bitcast.17, s32[2,16]{1,0:T(2,128)} %bitcast.20, bf16[2,16]{1,0:T(2,128)(2,1)} %bitcast.21, f32[1,1024]{1,0:T(1,128)} %bitcast.18, bf16[8,128]{1,0:T(8,128)(2,1)} %bitcast.19, ...), custom_call_target="tpu_custom_call" | custom-call | tf_op jit(solution)/shard_map/layer/pallas_call | solution.py:645
  49.6 1.3 %store.1 = (bf16[16,1024]{1,0:T(8,128)(2,1)}, f32[16,2,128,128]{3,2,1,0:T(8,128)}) custom-call(bf16[16,1024]{1,0:T(8,128)(2,1)S(1)} %get-tuple-element.4.a_in, f32[16,2,128,128]{3,2,1,0:T(8,128)S(1)} %get-tuple-element.5.b_in), custom_call_target="tpu_custom_call" | custom-call | tf_op jit(solution)/shard_map/store/pallas_call | solution.py:702

commit v6 on v5

--- a/solution.py
+++ b/solution.py
@@ -477,7 +477,6 @@
     chunks[0].spread(0)
     chunks[2].spread(0)
     weights.start()
-    chunks[DENSE].go()
     z_far.wait_recv()
     pack(1)
     chunks[1].spread(0)
@@ -485,6 +484,7 @@
     chunks[2].go()
     weights.start()
     chunks[1].go()
+    chunks[DENSE].go()
 
     c_pe, c_rb, c_ra = {}, {}, {}
 
@@ -562,8 +562,8 @@
             dst[FD:] = jnp.zeros((32 - FD, H), BF16)
     before_act(DENSE)
     act(2)
+    act(DENSE)
     sum_second(0)
-    act(DENSE)
     sum_second(1)
     give_back(0, 1, 2, 6)
     sum_second(2)

time: 51 us -> 50.6 us (level)
  no operation moved by 1% of the time
where the time goes in v6:
time: 50.6 us; the launch traced here: 50.5 us
  Pallas kernels  49.9 us (99%)
  between operations  0.65 us (1%)
    pallas_call x1, Pallas kernels, body(): pl.pallas_call(kernel, out_shape=(pltpu.VMEM((R, H), BF16), pltpu.VMEM(st...  48.5 us
    pallas_call x1, Pallas kernels, body(): pl.pallas_call(store, out_shape=(jax.ShapeDtypeStruct((R, H), BF16), jax....  1.34 us

profile of v6, /device:TPU:1, one launch (start us, length us, event | category | flops | bytes accessed | tf_op | source)
XLA Modules:
  0.0 50.5 jit_solution(13626759159131970017)
XLA Ops:
  0.6 48.5 %layer.1 = (bf16[16,1024]{1,0:T(8,128)(2,1)S(1)}, f32[16,2,128,128]{3,2,1,0:T(8,128)S(1)}) custom-call(bf16[16,1024]{1,0:T(8,128)(2,1)} %tokens_h.1, f32[1,2048]{1,0:T(1,128)} %bitcast.17, s32[2,16]{1,0:T(2,128)} %bitcast.20, bf16[2,16]{1,0:T(2,128)(2,1)} %bitcast.21, f32[1,1024]{1,0:T(1,128)} %bitcast.18, bf16[8,128]{1,0:T(8,128)(2,1)} %bitcast.19, ...), custom_call_target="tpu_custom_call" | custom-call | tf_op jit(solution)/shard_map/layer/pallas_call | solution.py:645
  49.2 1.3 %store.1 = (bf16[16,1024]{1,0:T(8,128)(2,1)}, f32[16,2,128,128]{3,2,1,0:T(8,128)}) custom-call(bf16[16,1024]{1,0:T(8,128)(2,1)S(1)} %get-tuple-element.4.a_in, f32[16,2,128,128]{3,2,1,0:T(8,128)S(1)} %get-tuple-element.5.b_in), custom_call_target="tpu_custom_call" | custom-call | tf_op jit(solution)/shard_map/store/pallas_call | solution.py:702

commit v7 on v6

--- a/solution.py
+++ b/solution.py
@@ -491,13 +491,18 @@
     def before_act(c):
         n = CHUNKS[c]
         chunks[c].across.wait_recv()
-        pre = dot_t(xe[c][...].reshape(PLANE * n, H), enter[c][...].reshape(512, H))
-        pe_o[c][...] = pre
-        for b in range(SIDE):
-            for a in range(SIDE):
-                f = SIDE * b + a
-                pe_s[c][SIDE * a + b] = pre[f * n : (f + 1) * n].astype(BF16)
-        c_pe[c] = remote(pe_s[c], pe_r[c], partner)
+        x = xe[c][...].reshape(PLANE * n, H)
+        weights_in = enter[c][...].reshape(512, H)
+        c_pe[c] = Group(pe_r[c])
+        for half in (slice(0, 256), slice(256, 512)):
+            pre = dot_t(x, weights_in[half])
+            pe_o[c][:, half] = pre
+            for b in range(SIDE):
+                for a in range(SIDE):
+                    f = SIDE * b + a
+                    pe_s[c][SIDE * a + b, :, half] = pre[f * n : (f + 1) * n].astype(BF16)
+            lanes = pl.ds(half.start, 256)
+            c_pe[c].add(pe_s[c].at[:, :, lanes], pe_r[c].at[:, :, lanes], partner)
 
     def act(c):
         n = CHUNKS[c]

time: 50.6 us -> 50.6 us (level)
  no operation moved by 1% of the time
where the time goes in v7:
time: 50.6 us; the launch traced here: 50.5 us
  Pallas kernels  49.9 us (99%)
  between operations  0.65 us (1%)
    pallas_call x1, Pallas kernels, body(): pl.pallas_call(kernel, out_shape=(pltpu.VMEM((R, H), BF16), pltpu.VMEM(st...  48.6 us
    pallas_call x1, Pallas kernels, body(): pl.pallas_call(store, out_shape=(jax.ShapeDtypeStruct((R, H), BF16), jax....  1.34 us

profile of v7, /device:TPU:1, one launch (start us, length us, event | category | flops | bytes accessed | tf_op | source)
XLA Modules:
  0.0 50.5 jit_solution(6220192663761324717)
XLA Ops:
  0.6 48.6 %layer.1 = (bf16[16,1024]{1,0:T(8,128)(2,1)S(1)}, f32[16,2,128,128]{3,2,1,0:T(8,128)S(1)}) custom-call(bf16[16,1024]{1,0:T(8,128)(2,1)} %tokens_h.1, f32[1,2048]{1,0:T(1,128)} %bitcast.17, s32[2,16]{1,0:T(2,128)} %bitcast.20, bf16[2,16]{1,0:T(2,128)(2,1)} %bitcast.21, f32[1,1024]{1,0:T(1,128)} %bitcast.18, bf16[8,128]{1,0:T(8,128)(2,1)} %bitcast.19, ...), custom_call_target="tpu_custom_call" | custom-call | tf_op jit(solution)/shard_map/layer/pallas_call | solution.py:650
  49.2 1.3 %store.1 = (bf16[16,1024]{1,0:T(8,128)(2,1)}, f32[16,2,128,128]{3,2,1,0:T(8,128)}) custom-call(bf16[16,1024]{1,0:T(8,128)(2,1)S(1)} %get-tuple-element.4.a_in, f32[16,2,128,128]{3,2,1,0:T(8,128)S(1)} %get-tuple-element.5.b_in), custom_call_target="tpu_custom_call" | custom-call | tf_op jit(solution)/shard_map/store/pallas_call | solution.py:707
